TPU v7x, 512 devices: a whole 4x4x16 slice. The times are simulated.
512 devices in a mesh: ep: 32 (over z, core), tp: 16 (over y, x).
Axes of the slice: x: 4, y: 4, z: 16, core: 2. Of those that a mesh axis runs over, the one named last changes fastest.
Arguments:
- mixer_input_channels: bfloat16 [8192, 4096], P('ep', 'tp'), may hold values from -6 to 6
- input_state_projection: bfloat16 [8192, 4096], P('ep', 'tp'), may hold values from -6 to 6
- output_state_projection: bfloat16 [8192, 4096], P('ep', 'tp'), may hold values from -6 to 6
- output_gate_logits: bfloat16 [8192, 4096], P('ep', 'tp'), may hold values from -6 to 6
- step_size_logits: float32 [8192, 64], P('ep', 'tp'), may hold values from -4.4 to 2.9
- extra_log_decay: float32 [8192, 64], P('ep', 'tp'), may hold values from -2.1 to 0, as said below
- mixer_channel_taps: bfloat16 [4, 4096], P(None, 'tp'), may hold values from -3 to 3
- input_state_taps: bfloat16 [4, 4096], P(None, 'tp'), may hold values from -3 to 3
- output_state_taps: bfloat16 [4, 4096], P(None, 'tp'), may hold values from -3 to 3
- decay_rate_log: float32 [64], P('tp')
- head_skip_weight: float32 [64], P('tp'), may hold values from 0.1 to 1.9
- grouped_norm_gain: float32 [4096], P('tp'), may hold values from 0.1 to 1.9
- mixer_output_weight: bfloat16 [4096, 2048], P('tp'), may hold values from -0.09375 to 0.09375
- expert_input_tokens: bfloat16 [4096, 2048], P('ep'), may hold values from -6 to 6
- routing: int32 [4096, 2], P('ep'), may hold values from 0 to 31, all different within a row; in each aligned block of 128 rows (0 to 127, 128 to 255, ...) at most 10 rows name the same one
- router_chosen_scores: float32 [4096, 2], P('ep'), may hold values from 0.05 to 1
- expert_norm_gain: float32 [2048], replicated, may hold values from 0.1 to 1.9
- expert_gate_weight: bfloat16 [32, 2048, 2048], P('ep', None, 'tp'), may hold values from -0.125 to 0.125
- expert_up_weight: bfloat16 [32, 2048, 2048], P('ep', None, 'tp'), may hold values from -0.125 to 0.125
- expert_down_weight: bfloat16 [32, 2048, 2048], P('ep', 'tp'), may hold values from -0.125 to 0.125
Outputs:
- mixer_output_first: bfloat16 [8192, 2048], P('ep', 'tp')
- moe_out: bfloat16 [4096, 2048], P('ep', 'tp')
Inputs may be any that keep to these rules, and one draw needn't show every extreme that they name: `routing`: within the rows of one index of ep (aligned blocks of 128 rows) no expert is named more than 10 times, some expert exactly 10 times; a row names 2 different experts. `extra_log_decay`: zero at all but a few positions.
All inputs are finite; a program needn't handle non-finite values.
Results may differ from a plain program's by a relative error of at most 0.018.
Values may be sent and summed in bfloat16 or wider, within the bound.
No kernel may reach another device: no remote copies, remote signals or barrier semaphores. Data moves between devices by JAX's collectives and lax.ppermute only.
A program may use at most 64 MiB of HBM per device.

v0:
```python
import functools

import jax
import jax.numpy as jnp
from jax import lax
from jax.experimental import pallas as pl
from jax.experimental.pallas import tpu as pltpu
from jax.sharding import Mesh
from jax.sharding import PartitionSpec as P

HEAD_DIM = 64
STATE = 128
BLOCK = 128
CHIPS = "ep_0"
EP = (CHIPS, "core")
SLOTS = 16
NOTE = 16
VMEM = 16 << 20
WHOLE_VMEM = 60 << 20
F32 = jnp.float32
BF16 = jnp.bfloat16

eps = 1e-06


def iota(shape, dim):
    return lax.broadcasted_iota(jnp.int32, shape, dim)


def dot(a, b, ca=1, cb=0, precision=None):
    return lax.dot_general(
        a, b, (((ca,), (cb,)), ((), ())), precision=precision, preferred_element_type=F32
    )


def silu(x):
    return x * (1.0 / (1.0 + jnp.exp(-x)))


def softplus(x):
    return jnp.maximum(x, 0.0) + jnp.log1p(jnp.exp(-jnp.abs(x)))


def fetched(body, ins, outs, own, far, late):
    def whole(*refs):
        given, rest = list(refs[:ins]), refs[ins : ins + outs + own]
        held, sems = refs[ins + outs + own : -1], refs[-1]
        copies = {}
        for k, index in enumerate(far):
            source = given[index]
            if source.shape != held[k].shape:
                source = source.at[pl.ds(source.shape[0] - held[k].shape[0], held[k].shape[0]), :]
            copies[index] = pltpu.make_async_copy(source, held[k], sems.at[k])
            copies[index].start()
            given[index] = held[k]
        for index in far:
            if index not in late:
                copies[index].wait()
        body(*given, *rest, *(copies[index].wait for index in late))

    return whole


def kernel_call(body, outs, args, flops, scratch=(), far=(), late=(), tails=(), vmem=VMEM):
    size = sum(a.size * a.dtype.itemsize for a in args)
    size += sum(o.size * o.dtype.itemsize for o in outs)
    specs = [
        pl.BlockSpec(memory_space=pltpu.HBM if k in far else pltpu.VMEM) for k in range(len(args))
    ]
    scratch = list(scratch)
    if far:
        body = fetched(body, len(args), len(outs), len(scratch), far, late)
        for k in far:
            dims = (8, args[k].shape[1]) if k in tails else args[k].shape
            scratch.append(pltpu.VMEM(dims, args[k].dtype))
        scratch.append(pltpu.SemaphoreType.DMA((len(far),)))
    return pl.pallas_call(
        body,
        out_shape=outs,
        in_specs=specs,
        out_specs=[pl.BlockSpec(memory_space=pltpu.VMEM)] * len(outs),
        scratch_shapes=scratch,
        cost_estimate=pl.CostEstimate(flops=flops, bytes_accessed=size, transcendentals=0),
        compiler_params=pltpu.CompilerParams(vmem_limit_bytes=vmem),
    )(*args)


def shape(dims, kind):
    return jax.ShapeDtypeStruct(dims, kind)


def upright(ref):
    wide = jnp.concatenate([ref[...].astype(F32)] * (8 // ref.shape[0]), axis=0)
    return wide.T[:, : ref.shape[0]]


def slots_of(routing_ref):
    tokens = routing_ref.shape[1]
    expert = iota((tokens, 128), 1)
    named = upright(routing_ref).astype(jnp.int32)
    first = expert == named[:, 0:1]
    second = expert == named[:, 1:2]
    member = jnp.where(first | second, 1.0, 0.0).astype(BF16)
    earlier = jnp.where(iota((tokens, tokens), 0) > iota((tokens, tokens), 1), 1.0, 0.0)
    place = dot(earlier.astype(BF16), member) + (expert * SLOTS).astype(F32)
    return [
        jnp.sum(jnp.where(chosen, place, 0.0), axis=1, keepdims=True).astype(jnp.int32)
        for chosen in (first, second)
    ]


def log_decay_of(step_ref, extra_ref, rate_ref):
    step = softplus(upright(step_ref))
    return step, step * -jnp.exp(rate_ref[...]) + upright(extra_ref)


def dispatch_body(
    tok_ref, gain_ref, routing_ref, x_ref, b_ref, c_ref, out_ref, edge_ref
):
    tokens, model = tok_ref.shape
    rows = tok_ref[...].astype(F32)
    scale = lax.rsqrt(jnp.sum(rows * rows, axis=1, keepdims=True) * (1.0 / model) + eps)
    columns = pl.ds(pl.multiple_of(lax.axis_index("tp") * 128, 128), 128)
    own = (tok_ref[:, columns].astype(F32) * scale * gain_ref[:, columns]).astype(BF16)
    slots = slots_of(routing_ref)
    place = iota((tokens, out_ref.shape[0]), 1)
    pick = jnp.where((place == slots[0]) | (place == slots[1]), 1.0, 0.0).astype(BF16)
    out_ref[...] = dot(pick, own, 0, 0).astype(BF16)
    for k, ref in enumerate((x_ref, b_ref, c_ref)):
        edge_ref[8 * k : 8 * k + 8, :] = ref[...]


def spread_body(capacity, in_ref, out_ref):
    count = out_ref.shape[1]
    row = iota((count, in_ref.shape[0]), 0)
    source = row // capacity * SLOTS + row % capacity
    pick = jnp.where(iota(source.shape, 1) == source, 1.0, 0.0).astype(BF16)
    packed = dot(pick, in_ref[...]).astype(BF16)
    for peer in range(out_ref.shape[0]):
        out_ref[peer] = packed


def ffn_body(in_ref, gate_ref, up_ref, down_ref, out_ref, wait):
    parts, rows, width = in_ref.shape
    total = jnp.zeros((rows, 2 * width), F32)
    for k in range(0, parts, 2):
        left = jnp.concatenate([in_ref[k], in_ref[k + 1]], axis=1)
        span = pl.ds(k * width, 2 * width)
        right = jnp.concatenate([gate_ref[span, :], up_ref[span, :]], axis=1)
        total = total + dot(left, right)
    hidden = (silu(total[:, :width]) * total[:, width:]).astype(BF16)
    wait()
    for k in range(0, parts, 2):
        value = dot(hidden, down_ref[:, k * width : (k + 2) * width]).astype(BF16)
        out_ref[k] = value[:, :width]
        out_ref[k + 1] = value[:, width:]


def sum_of(in_ref):
    total = in_ref[0].astype(F32)
    for k in range(1, in_ref.shape[0]):
        total = total + in_ref[k].astype(F32)
    return total.astype(BF16)


def expert_sum_body(capacity, in_ref, out_ref):
    total = sum_of(in_ref)
    count = total.shape[0]
    row = iota((out_ref.shape[0], count), 0)
    source = jnp.where(row % SLOTS < capacity, row // SLOTS * capacity + row % SLOTS, -1)
    pick = jnp.where(iota(source.shape, 1) == source, 1.0, 0.0).astype(BF16)
    out_ref[...] = dot(pick, total).astype(BF16)


def sum_body(in_ref, out_ref):
    out_ref[...] = sum_of(in_ref)


def combine_body(table_ref, routing_ref, score_ref, out_ref):
    tokens = routing_ref.shape[1]
    scores = upright(score_ref)
    whole = scores[:, 0:1] + scores[:, 1:2]
    place = iota((tokens, table_ref.shape[0]), 1)
    total = jnp.zeros(out_ref.shape, F32)
    for index, slot in enumerate(slots_of(routing_ref)):
        pick = jnp.where(place == slot, 1.0, 0.0).astype(BF16)
        total = total + scores[:, index : index + 1] / whole * dot(pick, table_ref[...])
    out_ref[...] = total.astype(BF16)


def conv_silu(values_ref, prior_ref, taps_ref, start, held):
    length = values_ref.shape[0]
    reach = taps_ref.shape[0] - 1
    held[0:8, :] = prior_ref[start : start + 8, :].astype(F32)
    held[8 : 8 + length, :] = values_ref[...].astype(F32)
    total = jnp.zeros(values_ref.shape, F32)
    for k in range(reach + 1):
        total = total + held[8 - reach + k : 8 - reach + k + length, :] * taps_ref[
            k : k + 1, :
        ].astype(F32)
    return silu(total).astype(BF16)


def running_sum(values):
    length = values.shape[0]
    reach = 1
    row = iota(values.shape, 0)
    while reach < length:
        moved = pltpu.roll(values, reach, 0)
        values = values + jnp.where(row >= reach, moved, 0.0)
        reach *= 2
    return values


def pair(left, right, dims, dim):
    return jnp.where(iota(dims, dim) < HEAD_DIM, left, right)


def block_terms(block, step_all, log_all):
    rows = slice(block * BLOCK, (block + 1) * BLOCK)
    step = step_all[rows]
    decay = running_sum(log_all[rows])
    return rows, step, decay, decay[BLOCK - 1 : BLOCK, :]


def states_body(
    x_ref, b_ref, c_ref, prior_ref, xt_ref, bt_ref, ct_ref, step_ref, extra_ref, rate_ref,
    xo_ref, bo_ref, co_ref, first_ref, total_ref, held, wide_ref,
):
    xo_ref[...] = conv_silu(x_ref, prior_ref, xt_ref, 0, held)
    bo_ref[...] = conv_silu(b_ref, prior_ref, bt_ref, 8, held)
    co_ref[...] = conv_silu(c_ref, prior_ref, ct_ref, 16, held)
    step_all, log_all = log_decay_of(step_ref, extra_ref, rate_ref)
    wide = (BLOCK, 128)
    for group in range(x_ref.shape[1] // 128):
        columns = slice(group * 128, (group + 1) * 128)
        a, b = 2 * group, 2 * group + 1
        state = None
        for block in range(x_ref.shape[0] // BLOCK):
            rows, step, decay, last = block_terms(block, step_all, log_all)
            x = xo_ref[rows, columns].astype(F32)
            x_step = (x * pair(step[:, a : a + 1], step[:, b : b + 1], wide, 1)).astype(BF16)
            left = jnp.exp(last - decay)
            weighted = x_step.astype(F32) * pair(left[:, a : a + 1], left[:, b : b + 1], wide, 1)
            new = dot(weighted.astype(BF16), bo_ref[rows, columns], 0, 0)
            if state is None:
                first_ref[columns, :] = new
                state = new
            else:
                kept = jnp.exp(last)
                state = state * pair(kept[:, a : a + 1], kept[:, b : b + 1], wide, 0) + new
        total_ref[columns, :] = state.astype(BF16)
    write_log(total_ref, jnp.sum(log_all, axis=0, keepdims=True), wide_ref)


def write_log(ref, log, wide_ref):
    rows = ref.shape[0] - NOTE
    wide_ref[...] = jnp.zeros_like(wide_ref)
    for part in range(3):
        piece = log.astype(ref.dtype).astype(F32)
        wide_ref[part : part + 1, 0 : log.shape[1]] = piece
        log = log - piece
    ref[rows:, :] = wide_ref[...].astype(ref.dtype)


def by_row(values, rows):
    head = iota((rows, 128), 0) // HEAD_DIM
    total = jnp.broadcast_to(values[:, 0:1], (rows, 128))
    for k in range(1, values.shape[1]):
        total = jnp.where(head == k, values[:, k : k + 1], total)
    return total


def read(part):
    rows = part.shape[0] - NOTE
    note = part[rows:, :].astype(F32)
    log = (note[0:1] + note[1:2] + note[2:3])[:, : rows // HEAD_DIM]
    return part[:rows, :].astype(F32), log


def joined(earlier, later):
    decay = by_row(jnp.exp(later[1]), later[0].shape[0])
    return earlier[0] * decay + later[0], earlier[1] + later[1]


def write(ref, value, wide_ref):
    ref[: ref.shape[0] - NOTE, :] = value[0].astype(ref.dtype)
    write_log(ref, value[1], wide_ref)


def join_core_body(both_ref, out_ref, wide_ref):
    write(out_ref, joined(read(both_ref[0]), read(both_ref[1])), wide_ref)


def join_first_body(came_ref, own_ref, out_ref, wide_ref):
    write(out_ref, joined(read(came_ref[...]), read(own_ref[...])), wide_ref)


def join_body(came_ref, own_ref, before_ref, out_ref, new_ref, wide_ref):
    came = read(came_ref[...])
    write(out_ref, joined(came, read(own_ref[...])), wide_ref)
    write(new_ref, joined(came, read(before_ref[...])), wide_ref)


def income_of(came_ref, before_ref, both_ref):
    state = joined(read(came_ref[...]), read(before_ref[...]))
    inside = joined(state, read(both_ref[0]))
    return jnp.where(lax.axis_index("core") == 1, inside[0], state[0])


def mixer_body(
    x_ref, b_ref, c_ref, gate_ref, first_ref, came_ref, before_ref, both_ref, step_ref, extra_ref,
    rate_ref, skip_ref, gain_ref, weight_ref, out_ref, normed, income_ref,
):
    income_ref[...] = income_of(came_ref, before_ref, both_ref)
    step_all, log_all = log_decay_of(step_ref, extra_ref, rate_ref)
    wide = (BLOCK, 128)
    causal = iota(wide, 0) >= iota(wide, 1)
    for block in range(x_ref.shape[0] // BLOCK):
        rows, step, decay, last = block_terms(block, step_all, log_all)
        grown = jnp.exp(decay)
        for group in range(x_ref.shape[1] // 128):
            columns = slice(group * 128, (group + 1) * 128)
            a, b = 2 * group, 2 * group + 1
            x = x_ref[rows, columns].astype(F32)
            x_step = (x * pair(step[:, a : a + 1], step[:, b : b + 1], wide, 1)).astype(BF16)
            c = c_ref[rows, columns]
            inner = dot(c, b_ref[rows, columns], 1, 1)
            parts = []
            for head in (a, b):
                along = jnp.broadcast_to(decay[:, head : head + 1], wide)
                distance = along - along.T
                scale = jnp.where(causal, jnp.exp(jnp.where(causal, distance, 0.0)), 0.0)
                parts.append(dot((inner * scale).astype(BF16), x_step))
            y = pair(parts[0], parts[1], wide, 1)
            entering = income_ref[columns, :]
            if block > 0:
                entering = entering * pair(kept[:, a : a + 1], kept[:, b : b + 1], wide, 0)
                entering = entering + first_ref[columns, :]
            off = dot(c, entering.astype(BF16), 1, 1)
            off = off * pair(grown[:, a : a + 1], grown[:, b : b + 1], wide, 1)
            skip = pair(skip_ref[:, a : a + 1], skip_ref[:, b : b + 1], wide, 1)
            mixed = (y + off + skip * x) * silu(gate_ref[rows, columns].astype(F32))
            mean = jnp.sum(mixed * mixed, axis=1, keepdims=True) * (1.0 / 128)
            mixed = mixed * lax.rsqrt(mean + eps) * gain_ref[:, columns]
            normed[rows, columns] = mixed.astype(BF16)
        kept = jnp.exp(last)
    for k in range(0, out_ref.shape[0], 2):
        value = dot(normed[...], weight_ref[:, k * 128 : (k + 2) * 128]).astype(BF16)
        out_ref[k] = value[:, :128]
        out_ref[k + 1] = value[:, 128:]


def all_to_all(value, axis):
    return lax.all_to_all(value, axis, split_axis=0, concat_axis=0, tiled=True)


def per_device(
    mixer_input_channels,
    input_state_projection,
    output_state_projection,
    output_gate_logits,
    step_size_logits,
    extra_log_decay,
    mixer_channel_taps,
    input_state_taps,
    output_state_taps,
    decay_rate_log,
    head_skip_weight,
    grouped_norm_gain,
    mixer_output_weight,
    expert_input_tokens,
    routing,
    router_chosen_scores,
    expert_norm_gain,
    expert_gate_weight,
    expert_up_weight,
    expert_down_weight,
):
    parts = lax.axis_size("tp")
    devices = lax.axis_size(EP)
    length, channels = mixer_input_channels.shape
    tokens, model = expert_input_tokens.shape
    top = routing.shape[1]
    capacity = (tokens * top * 5 + 4 * devices - 1) // (4 * devices)
    slots = devices * SLOTS
    rate, skip = decay_rate_log[None], head_skip_weight[None]
    step_rows, extra_rows = step_size_logits.T, extra_log_decay.T
    routing_rows = routing.T

    outgoing, edge = kernel_call(
        dispatch_body,
        [shape((slots, 128), BF16), shape((24, channels), BF16)],
        (
            expert_input_tokens, expert_norm_gain[None], routing_rows,
            mixer_input_channels, input_state_projection, output_state_projection,
        ),
        2 * slots * tokens * 128,
        far=(0, 1, 2, 3, 4, 5),
        tails=(3, 4, 5),
        vmem=WHOLE_VMEM,
    )
    prior = lax.ppermute(edge, EP, [(i, i + 1) for i in range(devices - 1)])
    arrived = all_to_all(outgoing.reshape(devices, SLOTS, 128), EP)
    arrived = arrived.reshape(slots, 128)

    note = channels + NOTE
    wide = pltpu.VMEM((NOTE, 128), F32)
    x_conv, b_conv, c_conv, first, total = kernel_call(
        states_body,
        [shape((length, channels), BF16)] * 3
        + [shape((channels, STATE), F32), shape((note, STATE), BF16)],
        (
            mixer_input_channels, input_state_projection, output_state_projection, prior,
            mixer_channel_taps, input_state_taps, output_state_taps,
            step_rows, extra_rows, rate,
        ),
        2 * length * channels * STATE,
        [pltpu.VMEM((length + 8, channels), F32), wide],
        far=(0, 1, 2, 4, 5, 6, 7, 8, 9),
        vmem=WHOLE_VMEM,
    )

    def moved(value, distance):
        chips = lax.axis_size(CHIPS)
        route = [(i, i + distance) for i in range(chips - distance)]
        return lax.ppermute(value, CHIPS, route)

    def join(body, values, more=()):
        outs = [shape((note, STATE), BF16), *more]
        return kernel_call(body, outs, values, 4 * channels * STATE, [wide])

    both = lax.all_gather(total, "core")
    (upto,) = join(join_core_body, (both,))
    before = came = moved(upto, 1)
    (upto,) = join(join_first_body, (came, upto))
    for distance in (2, 4):
        came = moved(upto, distance)
        upto, before = join(join_body, (came, upto, before), [shape((note, STATE), F32)])
    came = moved(upto, 8)

    (copies,) = kernel_call(
        functools.partial(spread_body, capacity),
        [shape((parts, devices * capacity, 128), BF16)],
        (arrived,),
        2 * slots * devices * capacity * 128,
    )
    gathered = all_to_all(copies, "tp")

    (partial_rows,) = kernel_call(
        ffn_body,
        [shape((parts, devices * capacity, 128), BF16)],
        (gathered, expert_gate_weight[0], expert_up_weight[0], expert_down_weight[0]),
        6 * devices * capacity * model * 128,
        far=(3,),
        late=(3,),
    )
    expert_parts = all_to_all(partial_rows, "tp")

    (mixer_part,) = kernel_call(
        mixer_body,
        [shape((parts, length, 128), BF16)],
        (
            x_conv, b_conv, c_conv, output_gate_logits, first, came, before, both,
            step_rows, extra_rows, rate, skip, grouped_norm_gain[None], mixer_output_weight,
        ),
        2 * length * channels * model,
        [pltpu.VMEM((length, channels), BF16), pltpu.VMEM((channels, STATE), F32)],
    )
    mixer_parts = all_to_all(mixer_part, "tp")

    (back,) = kernel_call(
        functools.partial(expert_sum_body, capacity),
        [shape((slots, 128), BF16)],
        (expert_parts,),
        2 * slots * devices * capacity * 128,
    )
    table = all_to_all(back.reshape(devices, SLOTS, 128), EP).reshape(slots, 128)

    (mixer_output_first,) = kernel_call(
        sum_body, [shape((length, 128), BF16)], (mixer_parts,), parts * length * 128
    )
    (moe_out,) = kernel_call(
        combine_body,
        [shape((tokens, 128), BF16)],
        (table, routing_rows, router_chosen_scores.T),
        4 * tokens * slots * 128,
    )
    return (mixer_output_first, moe_out)


def solution(mesh):
    split = Mesh(mesh.devices.reshape(16, 2, mesh.shape["tp"]), (*EP, "tp"))
    in_specs = (
        P(EP, "tp"),
        P(EP, "tp"),
        P(EP, "tp"),
        P(EP, "tp"),
        P(EP, "tp"),
        P(EP, "tp"),
        P(None, "tp"),
        P(None, "tp"),
        P(None, "tp"),
        P("tp"),
        P("tp"),
        P("tp"),
        P("tp", None),
        P(EP, None),
        P(EP, None),
        P(EP, None),
        P(),
        P(EP, None, "tp"),
        P(EP, None, "tp"),
        P(EP, "tp", None),
    )
    out_specs = (P(EP, "tp"), P(EP, "tp"))
    return jax.shard_map(
        per_device, mesh=split, in_specs=in_specs, out_specs=out_specs, check_vma=False
    )
```

profile of v0, /device:TPU:1, one launch (start us, length us, event | category | flops | bytes accessed | tf_op | source)
XLA Modules:
  0.0 177.0 jit_solution(1639266095618739165)
XLA Ops:
  0.6 2.4 %shard_map.203 = (bf16[512,128]{1,0:T(8,128)(2,1)}, bf16[24,256]{1,0:T(8,128)(2,1)}) custom-call(bf16[128,2048]{1,0:T(8,128)(2,1)} %refs_0_.2, f32[1,2048]{1,0:T(1,128)} %bitcast.35, s32[2,128]{1,0:T(2,128)} %bitcast.27, bf16[256,256]{1,0:T(8,128)(2,1)} %refs_0_.3, bf16[256,256]{1,0:T(8,128)(2,1)} %refs_1_.1, bf16[256,256]{1,0:T(8,128)(2,1)} %refs_2_.1), custom_call_target="tpu_custom_call" | custom-call | flops 16777216 | bytes 1070080 | tf_op jit(solution)/shard_map/pallas_call | solution.py:77
  3.1 32.6 %all_to_all.25 = bf16[32,16,128]{2,1,0:T(8,128)(2,1)S(1)} all-to-all(bf16[32,16,128]{2,1,0:T(8,128)(2,1)} %bitcast.34), channel_id=1, replica_groups=mesh['ep_0'=16,'core'=2,'tp'=16] {'ep_0','core'}, dimensions={0} | all-to-all | bytes 262144 | tf_op jit(solution)/shard_map/all_to_all | solution.py:355
  36.0 24.8 %all_to_all.26.refs_0_ = bf16[16,320,128]{2,1,0:T(8,128)(2,1)S(1)} all-to-all(bf16[16,320,128]{2,1,0:T(8,128)(2,1)S(1)} %shard_map.211), channel_id=1, replica_groups=mesh['ep_0'=16,'core'=2,'tp'=16] {'tp'}, dimensions={0} | all-to-all | bytes 2621440 | tf_op jit(solution)/shard_map/all_to_all | solution.py:355
  60.8 2.8 %shard_map.212 = bf16[16,320,128]{2,1,0:T(8,128)(2,1)} custom-call(bf16[16,320,128]{2,1,0:T(8,128)(2,1)S(1)} %all_to_all.26.refs_0_, bf16[2048,128]{1,0:T(8,128)(2,1)S(1)} %bitcast.20, bf16[2048,128]{1,0:T(8,128)(2,1)S(1)} %bitcast.21, bf16[128,2048]{1,0:T(8,128)(2,1)S(1)} %bitcast.22), custom_call_target="tpu_custom_call" | custom-call | flops 503316480 | bytes 4194304 | tf_op jit(solution)/shard_map/pallas_call | solution.py:77
  63.6 3.7 %all-to-all-start.3 = ((bf16[16,320,128]{2,1,0:T(8,128)(2,1)}), bf16[16,320,128]{2,1,0:T(8,128)(2,1)S(1)}, u32[]{:S(2)}, u32[]{:S(2)}) async-start(bf16[16,320,128]{2,1,0:T(8,128)(2,1)} %shard_map.212), calls=%async_computation.3 | async-start | bytes 2621440 | tf_op jit(solution)/shard_map/all_to_all | solution.py:355
  67.4 4.8 %collective-permute-start = (bf16[24,256]{1,0:T(8,128)(2,1)S(1)}, bf16[24,256]{1,0:T(8,128)(2,1)S(1)}, u32[]{:S(2)}, u32[]{:S(2)}) collective-permute-start(bf16[24,256]{1,0:T(8,128)(2,1)S(1)} %copy-done.17), channel_id=1, source_target_pairs={{0,16},{16,32},{32,48},{48,64},{64,80},{80,96},{96,112},{112,128},... | collective-permute-start | bytes 36872 | tf_op jit(solution)/shard_map/ppermute | solution.py:403
  73.6 3.7 %shard_map.204 = (bf16[256,256]{1,0:T(8,128)(2,1)}, bf16[256,256]{1,0:T(8,128)(2,1)}, bf16[256,256]{1,0:T(8,128)(2,1)}, f32[256,128]{1,0:T(8,128)}, bf16[272,128]{1,0:T(8,128)(2,1)}) custom-call(bf16[256,256]{1,0:T(8,128)(2,1)} %refs_0_.3, bf16[256,256]{1,0:T(8,128)(2,1)} %refs_1_.1, bf16[256,256]{1,0:T(8,128)(2,1)} %refs_2_.1, bf16[24,256]{1,0:T(8,128)(2,1)} %copy-done.16, ...), custom_call_target="tpu_custom_call" | custom-call | flops 16777216 | bytes 1013776 | tf_op jit(solution)/shard_map/pallas_call | solution.py:77
  77.3 2.1 %all-gather = bf16[544,128]{1,0:T(8,128)(2,1)S(1)} all-gather(bf16[272,128]{1,0:T(8,128)(2,1)} %get-tuple-element.18), channel_id=2, replica_groups=mesh['ep_0'=16,'core'=2,'tp'=16] {'core'}, dimensions={0}, use_global_device_ids=true | all-gather | bytes 208896 | tf_op jit(solution)/shard_map/all_gather | solution.py:433
  79.6 4.0 %collective-permute-start.1 = (bf16[272,128]{1,0:T(8,128)(2,1)S(1)}, bf16[272,128]{1,0:T(8,128)(2,1)S(1)}, u32[]{:S(2)}, u32[]{:S(2)}) collective-permute-start(bf16[272,128]{1,0:T(8,128)(2,1)S(1)} %shard_map.205.own_ref), channel_id=1, source_target_pairs={{0,32},{32,64},{64,96},{96,128},{128,160},{160,192},{192,224},{224... | collective-permute-start | bytes 208904 | tf_op jit(solution)/shard_map/ppermute | solution.py:427
  83.5 1.3 collective-permute-done.1.came_ref.before_ref
  85.0 4.6 %collective-permute-start.2 = (bf16[272,128]{1,0:T(8,128)(2,1)S(1)}, bf16[272,128]{1,0:T(8,128)(2,1)S(1)}, u32[]{:S(2)}, u32[]{:S(2)}) collective-permute-start(bf16[272,128]{1,0:T(8,128)(2,1)S(1)} %shard_map.206.own_ref), channel_id=1, source_target_pairs={{0,64},{32,96},{64,128},{96,160},{128,192},{160,224},{192,256},{22... | collective-permute-start | bytes 208904 | tf_op jit(solution)/shard_map/ppermute | solution.py:427
  89.6 1.3 collective-permute-done.2.came_ref
  91.1 9.7 %collective-permute-start.3 = (bf16[272,128]{1,0:T(8,128)(2,1)S(1)}, bf16[272,128]{1,0:T(8,128)(2,1)S(1)}, u32[]{:S(2)}, u32[]{:S(2)}) collective-permute-start(bf16[272,128]{1,0:T(8,128)(2,1)S(1)} %get-tuple-element.19.own_ref), channel_id=1, source_target_pairs={{0,128},{32,160},{64,192},{96,224},{128,256},{160,288},{192,320},{... | collective-permute-start | bytes 208904 | tf_op jit(solution)/shard_map/ppermute | solution.py:427
  100.8 1.3 collective-permute-done.3.came_ref
  102.3 12.4 %collective-permute-start.4 = (bf16[272,128]{1,0:T(8,128)(2,1)S(1)}, bf16[272,128]{1,0:T(8,128)(2,1)S(1)}, u32[]{:S(2)}, u32[]{:S(2)}) collective-permute-start(bf16[272,128]{1,0:T(8,128)(2,1)S(1)} %get-tuple-element.21), channel_id=1, source_target_pairs={{0,256},{32,288},{64,320},{96,352},{128,384},{160,416},{192,448},{... | collective-permute-start | bytes 208904 | tf_op jit(solution)/shard_map/ppermute | solution.py:427
  114.7 1.3 collective-permute-done.4.came_ref
  117.0 0.9 copy-done.6
  119.7 3.0 %shard_map.209 = bf16[16,256,128]{2,1,0:T(8,128)(2,1)} custom-call(bf16[256,256]{1,0:T(8,128)(2,1)S(1)} %copy-done.5, bf16[256,256]{1,0:T(8,128)(2,1)S(1)} %copy-done.6, bf16[256,256]{1,0:T(8,128)(2,1)S(1)} %copy-done.7, bf16[256,256]{1,0:T(8,128)(2,1)S(1)} %copy-done.4, f32[256,128]{1,0:T(8,128)S(1)} %copy-done.8, ...), custom_call_target="tpu_custom_call" | custom-call | flops 268435456 | bytes 3109920 | tf_op jit(solution)/shard_map/pallas_call | solution.py:77
  122.7 5.8 %all-to-all-start = ((bf16[16,256,128]{2,1,0:T(8,128)(2,1)}), bf16[16,256,128]{2,1,0:T(8,128)(2,1)S(1)}, u32[]{:S(2)}, u32[]{:S(2)}) async-start(bf16[16,256,128]{2,1,0:T(8,128)(2,1)} %shard_map.209), calls=%async_computation | async-start | bytes 2097152 | tf_op jit(solution)/shard_map/all_to_all | solution.py:355
  128.6 1.1 shard_map.213
  129.6 13.9 %all-to-all-done.in_ref = bf16[16,256,128]{2,1,0:T(8,128)(2,1)S(1)} async-done(((bf16[16,256,128]{2,1,0:T(8,128)(2,1)}), bf16[16,256,128]{2,1,0:T(8,128)(2,1)S(1)}, u32[]{:S(2)}, u32[]{:S(2)}) %all-to-all-start) | async-done | bytes 1048608 | tf_op jit(solution)/shard_map/all_to_all | solution.py:355
  143.5 16.2 %all-to-all-start.4 = ((bf16[32,16,128]{2,1,0:T(8,128)(2,1)}), bf16[32,16,128]{2,1,0:T(8,128)(2,1)S(1)}, u32[]{:S(2)}, u32[]{:S(2)}) async-start(bf16[32,16,128]{2,1,0:T(8,128)(2,1)} %bitcast.13), calls=%async_computation.4 | async-start | bytes 262144 | tf_op jit(solution)/shard_map/all_to_all | solution.py:355
  160.6 15.1 %all-to-all-done.4 = bf16[32,16,128]{2,1,0:T(8,128)(2,1)S(1)} async-done(((bf16[32,16,128]{2,1,0:T(8,128)(2,1)}), bf16[32,16,128]{2,1,0:T(8,128)(2,1)S(1)}, u32[]{:S(2)}, u32[]{:S(2)}) %all-to-all-start.4) | async-done | bytes 131104 | tf_op jit(solution)/shard_map/all_to_all | solution.py:355
  175.6 1.4 shard_map.214
  (43 shorter events, 5.8 us)
Async XLA Ops:
  35.9 24.8 %copy-start.1 = (bf16[1,2048,128]{2,1,0:T(8,128)(2,1)S(1)}, bf16[1,2048,128]{2,1,0:T(8,128)(2,1)}, u32[]{:S(2)}) copy-start(bf16[1,2048,128]{2,1,0:T(8,128)(2,1)} %param.37) | copy-start | bytes 1572868
  36.0 24.8 %copy-start.2 = (bf16[1,2048,128]{2,1,0:T(8,128)(2,1)S(1)}, bf16[1,2048,128]{2,1,0:T(8,128)(2,1)}, u32[]{:S(2)}) copy-start(bf16[1,2048,128]{2,1,0:T(8,128)(2,1)} %param.38) | copy-start | bytes 1572868
  36.0 24.8 %copy-start.3 = (bf16[1,128,2048]{2,1,0:T(8,128)(2,1)S(1)}, bf16[1,128,2048]{2,1,0:T(8,128)(2,1)}, u32[]{:S(2)}) copy-start(bf16[1,128,2048]{2,1,0:T(8,128)(2,1)} %param.39) | copy-start | bytes 1572868
  63.6 3.8 %copy-start.17 = (bf16[24,256]{1,0:T(8,128)(2,1)S(1)}, bf16[24,256]{1,0:T(8,128)(2,1)}, u32[]{:S(2)}) copy-start(bf16[24,256]{1,0:T(8,128)(2,1)} %get-tuple-element.13) | copy-start | bytes 36868
  63.6 59.2 %all-to-all-start.3 = ((bf16[16,320,128]{2,1,0:T(8,128)(2,1)}), bf16[16,320,128]{2,1,0:T(8,128)(2,1)S(1)}, u32[]{:S(2)}, u32[]{:S(2)}) async-start(bf16[16,320,128]{2,1,0:T(8,128)(2,1)} %shard_map.212), calls=%async_computation.3 | async-start | bytes 2621440 | tf_op jit(solution)/shard_map/all_to_all | solution.py:355
  67.3 48.7 %copy-start = (bf16[256,2048]{1,0:T(8,128)(2,1)S(1)}, bf16[256,2048]{1,0:T(8,128)(2,1)}, u32[]{:S(2)}) copy-start(bf16[256,2048]{1,0:T(8,128)(2,1)} %weight_ref.1) | copy-start | bytes 3145732
  67.3 48.7 %copy-start.4 = (bf16[256,256]{1,0:T(8,128)(2,1)S(1)}, bf16[256,256]{1,0:T(8,128)(2,1)}, u32[]{:S(2)}) copy-start(bf16[256,256]{1,0:T(8,128)(2,1)} %gate_ref.1) | copy-start | bytes 393220
  67.3 48.7 %copy-start.9 = (f32[256,4]{0,1:T(4,128)S(1)}, f32[256,4]{0,1:T(4,128)}, u32[]{:S(2)}) copy-start(f32[256,4]{0,1:T(4,128)} %param.24) | copy-start | bytes 12292
  67.3 48.7 %copy-start.10 = (f32[256,4]{0,1:T(4,128)S(1)}, f32[256,4]{0,1:T(4,128)}, u32[]{:S(2)}) copy-start(f32[256,4]{0,1:T(4,128)} %param.25) | copy-start | bytes 12292
  67.3 48.7 %copy-start.12 = (f32[4]{0:T(128)S(1)}, f32[4]{0:T(128)}, u32[]{:S(2)}) copy-start(f32[4]{0:T(128)} %param.29) | copy-start | bytes 52
  67.4 48.7 %copy-start.13 = (f32[256]{0:T(256)S(1)}, f32[256]{0:T(256)}, u32[]{:S(2)}) copy-start(f32[256]{0:T(256)} %param.31) | copy-start | bytes 3076
  67.4 48.7 %copy-start.15 = (f32[4]{0:T(128)S(1)}, f32[4]{0:T(128)}, u32[]{:S(2)}) copy-start(f32[4]{0:T(128)} %param.30) | copy-start | bytes 52
  67.4 5.6 %collective-permute-start = (bf16[24,256]{1,0:T(8,128)(2,1)S(1)}, bf16[24,256]{1,0:T(8,128)(2,1)S(1)}, u32[]{:S(2)}, u32[]{:S(2)}) collective-permute-start(bf16[24,256]{1,0:T(8,128)(2,1)S(1)} %copy-done.17), channel_id=1, source_target_pairs={{0,16},{16,32},{32,48},{48,64},{64,80},{80,96},{96,112},{112,128},... | collective-permute-start | bytes 36872 | tf_op jit(solution)/shard_map/ppermute | solution.py:403
  79.6 5.3 %collective-permute-start.1 = (bf16[272,128]{1,0:T(8,128)(2,1)S(1)}, bf16[272,128]{1,0:T(8,128)(2,1)S(1)}, u32[]{:S(2)}, u32[]{:S(2)}) collective-permute-start(bf16[272,128]{1,0:T(8,128)(2,1)S(1)} %shard_map.205.own_ref), channel_id=1, source_target_pairs={{0,32},{32,64},{64,96},{96,128},{128,160},{160,192},{192,224},{224... | collective-permute-start | bytes 208904 | tf_op jit(solution)/shard_map/ppermute | solution.py:427
  85.0 5.9 %collective-permute-start.2 = (bf16[272,128]{1,0:T(8,128)(2,1)S(1)}, bf16[272,128]{1,0:T(8,128)(2,1)S(1)}, u32[]{:S(2)}, u32[]{:S(2)}) collective-permute-start(bf16[272,128]{1,0:T(8,128)(2,1)S(1)} %shard_map.206.own_ref), channel_id=1, source_target_pairs={{0,64},{32,96},{64,128},{96,160},{128,192},{160,224},{192,256},{22... | collective-permute-start | bytes 208904 | tf_op jit(solution)/shard_map/ppermute | solution.py:427
  91.1 11.0 %collective-permute-start.3 = (bf16[272,128]{1,0:T(8,128)(2,1)S(1)}, bf16[272,128]{1,0:T(8,128)(2,1)S(1)}, u32[]{:S(2)}, u32[]{:S(2)}) collective-permute-start(bf16[272,128]{1,0:T(8,128)(2,1)S(1)} %get-tuple-element.19.own_ref), channel_id=1, source_target_pairs={{0,128},{32,160},{64,192},{96,224},{128,256},{160,288},{192,320},{... | collective-permute-start | bytes 208904 | tf_op jit(solution)/shard_map/ppermute | solution.py:427
  102.3 13.7 %collective-permute-start.4 = (bf16[272,128]{1,0:T(8,128)(2,1)S(1)}, bf16[272,128]{1,0:T(8,128)(2,1)S(1)}, u32[]{:S(2)}, u32[]{:S(2)}) collective-permute-start(bf16[272,128]{1,0:T(8,128)(2,1)S(1)} %get-tuple-element.21), channel_id=1, source_target_pairs={{0,256},{32,288},{64,320},{96,352},{128,384},{160,416},{192,448},{... | collective-permute-start | bytes 208904 | tf_op jit(solution)/shard_map/ppermute | solution.py:427
  116.1 0.9 copy-start.5
  117.9 0.9 copy-start.7
  118.8 0.9 copy-start.8
  122.7 20.8 %all-to-all-start = ((bf16[16,256,128]{2,1,0:T(8,128)(2,1)}), bf16[16,256,128]{2,1,0:T(8,128)(2,1)S(1)}, u32[]{:S(2)}, u32[]{:S(2)}) async-start(bf16[16,256,128]{2,1,0:T(8,128)(2,1)} %shard_map.209), calls=%async_computation | async-start | bytes 2097152 | tf_op jit(solution)/shard_map/all_to_all | solution.py:355
  128.6 47.1 %copy-start.11 = (s32[128,2]{0,1:T(2,128)S(1)}, s32[128,2]{0,1:T(2,128)}, u32[]{:S(2)}) copy-start(s32[128,2]{0,1:T(2,128)} %param.34) | copy-start | bytes 3076
  128.6 47.1 %copy-start.14 = (f32[128,2]{0,1:T(2,128)S(1)}, f32[128,2]{0,1:T(2,128)}, u32[]{:S(2)}) copy-start(f32[128,2]{0,1:T(2,128)} %param.35) | copy-start | bytes 3076
  143.5 32.1 %all-to-all-start.4 = ((bf16[32,16,128]{2,1,0:T(8,128)(2,1)}), bf16[32,16,128]{2,1,0:T(8,128)(2,1)S(1)}, u32[]{:S(2)}, u32[]{:S(2)}) async-start(bf16[32,16,128]{2,1,0:T(8,128)(2,1)} %bitcast.13), calls=%async_computation.4 | async-start | bytes 262144 | tf_op jit(solution)/shard_map/all_to_all | solution.py:355
  (2 other events, 1.5 us)
where the time goes:
time: 178 us; the launch traced here: 177 us
  starting transfers between devices  61.1 us (34%)
  blocking collectives  59.5 us (33%)
  waiting for transfers between devices  35.2 us (20%)
  Pallas kernels  16 us (9%)
  local copies, waits for them, and re-layouts  4.29 us (2%)
    all_to_all x2, blocking collectives, all_to_all(): return lax.all_to_all(value, axis, split_axis=0, concat_axis=0, tiled=True)  57.4 us
    ppermute x4, starting transfers between devices, moved(): return lax.ppermute(value, CHIPS, route)  30.6 us
    all_to_all x3, waiting for transfers between devices, all_to_all(): return lax.all_to_all(value, axis, split_axis=0, concat_axis=0, tiled=True)  29 us
    all_to_all x3, starting transfers between devices, all_to_all(): return lax.all_to_all(value, axis, split_axis=0, concat_axis=0, tiled=True)  25.8 us
    pallas_call x12, Pallas kernels, kernel_call(): pl.pallas_call(body, out_shape=outs, in_specs=specs, out_specs=[pl.BlockS...  16 us
    ppermute x4, waiting for transfers between devices, moved(): return lax.ppermute(value, CHIPS, route)  5.4 us
    ppermute x1, starting transfers between devices, per_device(): prior = lax.ppermute(edge, EP, [(i, i + 1) for i in range(devices - 1)])  4.77 us
    unnamed x36, local copies, waits for them, and re-layouts  4.29 us
  transfers between devices with their start and end apart: 8, of which 7 were waited for; matrix products, arithmetic and copies ran while one was open for 0% of the time, Pallas kernels for 5%

commit v1 on v0

--- a/solution.py
+++ b/solution.py
@@ -14,6 +14,7 @@
 CHIPS = "ep_0"
 EP = (CHIPS, "core")
 SLOTS = 16
+SIDE = 4
 NOTE = 16
 VMEM = 16 << 20
 WHOLE_VMEM = 60 << 20
@@ -170,10 +171,6 @@
     source = jnp.where(row % SLOTS < capacity, row // SLOTS * capacity + row % SLOTS, -1)
     pick = jnp.where(iota(source.shape, 1) == source, 1.0, 0.0).astype(BF16)
     out_ref[...] = dot(pick, total).astype(BF16)
-
-
-def sum_body(in_ref, out_ref):
-    out_ref[...] = sum_of(in_ref)
 
 
 def combine_body(table_ref, routing_ref, score_ref, out_ref):
@@ -310,8 +307,9 @@
 
 def mixer_body(
     x_ref, b_ref, c_ref, gate_ref, first_ref, came_ref, before_ref, both_ref, step_ref, extra_ref,
-    rate_ref, skip_ref, gain_ref, weight_ref, out_ref, normed, income_ref,
+    rate_ref, skip_ref, gain_ref, weight_ref, *rest,
 ):
+    outs, (normed, income_ref) = rest[:SIDE], rest[SIDE:]
     income_ref[...] = income_of(came_ref, before_ref, both_ref)
     step_all, log_all = log_decay_of(step_ref, extra_ref, rate_ref)
     wide = (BLOCK, 128)
@@ -345,10 +343,33 @@
             mixed = mixed * lax.rsqrt(mean + eps) * gain_ref[:, columns]
             normed[rows, columns] = mixed.astype(BF16)
         kept = jnp.exp(last)
-    for k in range(0, out_ref.shape[0], 2):
-        value = dot(normed[...], weight_ref[:, k * 128 : (k + 2) * 128]).astype(BF16)
-        out_ref[k] = value[:, :128]
-        out_ref[k + 1] = value[:, 128:]
+    y, x = lax.axis_index("tp") // SIDE, lax.axis_index("tp") % SIDE
+
+    def columns_of(up, across):
+        part = (y + up) % SIDE * SIDE + (x + across) % SIDE
+        return weight_ref[:, pl.ds(pl.multiple_of(part * 128, 128), 128)]
+
+    for across, out_ref in enumerate(outs):
+        for up in range(0, SIDE, 2):
+            both = jnp.concatenate([columns_of(up, across), columns_of(up + 1, across)], axis=1)
+            value = dot(normed[...], both).astype(BF16)
+            out_ref[up] = value[:, :128]
+            out_ref[up + 1] = value[:, 128:]
+
+
+def across_body(*refs):
+    for up in range(SIDE):
+        total = refs[0][up].astype(F32)
+        for k in range(1, SIDE):
+            total = total + refs[k][up].astype(F32)
+        refs[SIDE + up][...] = total.astype(BF16)
+
+
+def upward_body(*refs):
+    total = refs[0][...].astype(F32)
+    for k in range(1, SIDE):
+        total = total + refs[k][...].astype(F32)
+    refs[SIDE][...] = total.astype(BF16)
 
 
 def all_to_all(value, axis):
@@ -457,9 +478,9 @@
     )
     expert_parts = all_to_all(partial_rows, "tp")
 
-    (mixer_part,) = kernel_call(
+    mixer_parts = kernel_call(
         mixer_body,
-        [shape((parts, length, 128), BF16)],
+        [shape((SIDE, length, 128), BF16)] * SIDE,
         (
             x_conv, b_conv, c_conv, output_gate_logits, first, came, before, both,
             step_rows, extra_rows, rate, skip, grouped_norm_gain[None], mixer_output_weight,
@@ -467,7 +488,6 @@
         2 * length * channels * model,
         [pltpu.VMEM((length, channels), BF16), pltpu.VMEM((channels, STATE), F32)],
     )
-    mixer_parts = all_to_all(mixer_part, "tp")
 
     (back,) = kernel_call(
         functools.partial(expert_sum_body, capacity),
@@ -477,8 +497,24 @@
     )
     table = all_to_all(back.reshape(devices, SLOTS, 128), EP).reshape(slots, 128)
 
+    def passed(value, up, across):
+        route = [
+            (y * SIDE + x, (y + up) % SIDE * SIDE + (x + across) % SIDE)
+            for y in range(SIDE)
+            for x in range(SIDE)
+        ]
+        return lax.ppermute(value, "tp", route)
+
+    came = [passed(mixer_parts[k], 0, k) for k in range(1, SIDE)]
+    mixer_parts = kernel_call(
+        across_body,
+        [shape((length, 128), BF16)] * SIDE,
+        (mixer_parts[0], *came),
+        parts * length * 128,
+    )
+    came = [passed(mixer_parts[k], k, 0) for k in range(1, SIDE)]
     (mixer_output_first,) = kernel_call(
-        sum_body, [shape((length, 128), BF16)], (mixer_parts,), parts * length * 128
+        upward_body, [shape((length, 128), BF16)], (mixer_parts[0], *came), SIDE * length * 128
     )
     (moe_out,) = kernel_call(
         combine_body,

time: 178 us -> 166 us (0.933)
  the two profiles are of different devices: /device:TPU:1 before, /device:TPU:386 now
where the time goes in v1:
time: 166 us; the launch traced here: 165 us
  waiting for transfers between devices  51.7 us (31%)
  blocking collectives  50.4 us (30%)
  starting transfers between devices  46.2 us (28%)
  Pallas kernels  15.1 us (9%)
    all_to_all x2, blocking collectives, all_to_all(): return lax.all_to_all(value, axis, split_axis=0, concat_axis=0, tiled=True)  48.3 us
    ppermute x4, waiting for transfers between devices, moved(): return lax.ppermute(value, CHIPS, route)  35.1 us
    ppermute x6, starting transfers between devices, passed(): return lax.ppermute(value, 'tp', route)  21.8 us
    all_to_all x2, starting transfers between devices, all_to_all(): return lax.all_to_all(value, axis, split_axis=0, concat_axis=0, tiled=True)  15.9 us
    pallas_call x13, Pallas kernels, kernel_call(): pl.pallas_call(body, out_shape=outs, in_specs=specs, out_specs=[pl.BlockS...  15.1 us
    ppermute x6, waiting for transfers between devices, passed(): return lax.ppermute(value, 'tp', route)  12.3 us
    ppermute x4, starting transfers between devices, moved(): return lax.ppermute(value, CHIPS, route)  6.56 us
    ppermute x1, waiting for transfers between devices, per_device(): prior = lax.ppermute(edge, EP, [(i, i + 1) for i in range(devices - 1)])  4.3 us
  transfers between devices with their start and end apart: 13, of which 8 were waited for; matrix products, arithmetic and copies ran while one was open for 0% of the time, Pallas kernels for 5%

profile of v1, /device:TPU:386, one launch (start us, length us, event | category | flops | bytes accessed | tf_op | source)
XLA Modules:
  0.0 165.1 jit_solution(11752618291807379642)
XLA Ops:
  0.6 2.4 %shard_map.203 = (bf16[512,128]{1,0:T(8,128)(2,1)}, bf16[24,256]{1,0:T(8,128)(2,1)}) custom-call(bf16[128,2048]{1,0:T(8,128)(2,1)} %refs_0_.2, f32[1,2048]{1,0:T(1,128)} %bitcast.35, s32[2,128]{1,0:T(2,128)} %bitcast.27, bf16[256,256]{1,0:T(8,128)(2,1)} %refs_0_.3, bf16[256,256]{1,0:T(8,128)(2,1)} %refs_1_.1, bf16[256,256]{1,0:T(8,128)(2,1)} %refs_2_.1), custom_call_target="tpu_custom_call" | custom-call | flops 16777216 | bytes 1070080 | tf_op jit(solution)/shard_map/pallas_call | solution.py:78
  3.1 22.2 %all_to_all.20 = bf16[32,16,128]{2,1,0:T(8,128)(2,1)S(1)} all-to-all(bf16[32,16,128]{2,1,0:T(8,128)(2,1)} %bitcast.34), channel_id=1, replica_groups=mesh['ep_0'=16,'core'=2,'tp'=16] {'ep_0','core'}, dimensions={0} | all-to-all | bytes 262144 | tf_op jit(solution)/shard_map/all_to_all | solution.py:376
  25.6 26.0 %all_to_all.21.refs_0_ = bf16[16,320,128]{2,1,0:T(8,128)(2,1)S(1)} all-to-all(bf16[16,320,128]{2,1,0:T(8,128)(2,1)S(1)} %shard_map.212), channel_id=1, replica_groups=mesh['ep_0'=16,'core'=2,'tp'=16] {'tp'}, dimensions={0} | all-to-all | bytes 2621440 | tf_op jit(solution)/shard_map/all_to_all | solution.py:376
  51.7 2.8 %shard_map.213 = bf16[16,320,128]{2,1,0:T(8,128)(2,1)} custom-call(bf16[16,320,128]{2,1,0:T(8,128)(2,1)S(1)} %all_to_all.21.refs_0_, bf16[2048,128]{1,0:T(8,128)(2,1)S(1)} %bitcast.20, bf16[2048,128]{1,0:T(8,128)(2,1)S(1)} %bitcast.21, bf16[128,2048]{1,0:T(8,128)(2,1)S(1)} %bitcast.22), custom_call_target="tpu_custom_call" | custom-call | flops 503316480 | bytes 4194304 | tf_op jit(solution)/shard_map/pallas_call | solution.py:78
  54.5 5.0 %all-to-all-start.2 = ((bf16[16,320,128]{2,1,0:T(8,128)(2,1)}), bf16[16,320,128]{2,1,0:T(8,128)(2,1)S(1)}, u32[]{:S(2)}, u32[]{:S(2)}) async-start(bf16[16,320,128]{2,1,0:T(8,128)(2,1)} %shard_map.213), calls=%async_computation.2 | async-start | bytes 2621440 | tf_op jit(solution)/shard_map/all_to_all | solution.py:376
  59.4 1.9 %collective-permute-start = (bf16[24,256]{1,0:T(8,128)(2,1)S(1)}, bf16[24,256]{1,0:T(8,128)(2,1)S(1)}, u32[]{:S(2)}, u32[]{:S(2)}) collective-permute-start(bf16[24,256]{1,0:T(8,128)(2,1)S(1)} %copy-done.17), channel_id=1, source_target_pairs={{0,16},{16,32},{32,48},{48,64},{64,80},{80,96},{96,112},{112,128},... | collective-permute-start | bytes 36872 | tf_op jit(solution)/shard_map/ppermute | solution.py:424
  61.3 4.3 %collective-permute-done.refs_3_ = bf16[24,256]{1,0:T(8,128)(2,1)S(1)} collective-permute-done((bf16[24,256]{1,0:T(8,128)(2,1)S(1)}, bf16[24,256]{1,0:T(8,128)(2,1)S(1)}, u32[]{:S(2)}, u32[]{:S(2)}) %collective-permute-start) | collective-permute-done | bytes 12320 | tf_op jit(solution)/shard_map/ppermute | solution.py:424
  66.2 3.7 %shard_map.204 = (bf16[256,256]{1,0:T(8,128)(2,1)}, bf16[256,256]{1,0:T(8,128)(2,1)}, bf16[256,256]{1,0:T(8,128)(2,1)}, f32[256,128]{1,0:T(8,128)}, bf16[272,128]{1,0:T(8,128)(2,1)}) custom-call(bf16[256,256]{1,0:T(8,128)(2,1)} %refs_0_.3, bf16[256,256]{1,0:T(8,128)(2,1)} %refs_1_.1, bf16[256,256]{1,0:T(8,128)(2,1)} %refs_2_.1, bf16[24,256]{1,0:T(8,128)(2,1)} %copy-done.16, ...), custom_call_target="tpu_custom_call" | custom-call | flops 16777216 | bytes 1013776 | tf_op jit(solution)/shard_map/pallas_call | solution.py:78
  70.0 2.1 %all-gather = bf16[544,128]{1,0:T(8,128)(2,1)S(1)} all-gather(bf16[272,128]{1,0:T(8,128)(2,1)} %get-tuple-element.26), channel_id=2, replica_groups=mesh['ep_0'=16,'core'=2,'tp'=16] {'core'}, dimensions={0}, use_global_device_ids=true | all-gather | bytes 208896 | tf_op jit(solution)/shard_map/all_gather | solution.py:454
  72.3 2.1 %collective-permute-start.1 = (bf16[272,128]{1,0:T(8,128)(2,1)S(1)}, bf16[272,128]{1,0:T(8,128)(2,1)S(1)}, u32[]{:S(2)}, u32[]{:S(2)}) collective-permute-start(bf16[272,128]{1,0:T(8,128)(2,1)S(1)} %shard_map.205.own_ref), channel_id=1, source_target_pairs={{0,32},{32,64},{64,96},{96,128},{128,160},{160,192},{192,224},{224... | collective-permute-start | bytes 208904 | tf_op jit(solution)/shard_map/ppermute | solution.py:448
  74.4 5.5 %collective-permute-done.1.came_ref.before_ref = bf16[272,128]{1,0:T(8,128)(2,1)S(1)} collective-permute-done((bf16[272,128]{1,0:T(8,128)(2,1)S(1)}, bf16[272,128]{1,0:T(8,128)(2,1)S(1)}, u32[]{:S(2)}, u32[]{:S(2)}) %collective-permute-start.1) | collective-permute-done | bytes 69664 | tf_op jit(solution)/shard_map/ppermute | solution.py:448
  83.0 11.0 %all-to-all-start.3 = ((bf16[32,16,128]{2,1,0:T(8,128)(2,1)}), bf16[32,16,128]{2,1,0:T(8,128)(2,1)S(1)}, u32[]{:S(2)}, u32[]{:S(2)}) async-start(bf16[32,16,128]{2,1,0:T(8,128)(2,1)} %bitcast.13), calls=%async_computation.3 | async-start | bytes 262144 | tf_op jit(solution)/shard_map/all_to_all | solution.py:376
  95.5 15.2 %collective-permute-done.3.came_ref = bf16[272,128]{1,0:T(8,128)(2,1)S(1)} collective-permute-done((bf16[272,128]{1,0:T(8,128)(2,1)S(1)}, bf16[272,128]{1,0:T(8,128)(2,1)S(1)}, u32[]{:S(2)}, u32[]{:S(2)}) %collective-permute-start.3) | collective-permute-done | bytes 69664 | tf_op jit(solution)/shard_map/ppermute | solution.py:448
  112.1 14.5 %collective-permute-done.4.came_ref = bf16[272,128]{1,0:T(8,128)(2,1)S(1)} collective-permute-done((bf16[272,128]{1,0:T(8,128)(2,1)S(1)}, bf16[272,128]{1,0:T(8,128)(2,1)S(1)}, u32[]{:S(2)}, u32[]{:S(2)}) %collective-permute-start.4) | collective-permute-done | bytes 69664 | tf_op jit(solution)/shard_map/ppermute | solution.py:448
  126.6 2.1 %shard_map.209 = (bf16[4,256,128]{2,1,0:T(8,128)(2,1)S(1)}, bf16[4,256,128]{2,1,0:T(8,128)(2,1)S(1)}, bf16[4,256,128]{2,1,0:T(8,128)(2,1)S(1)}, bf16[4,256,128]{2,1,0:T(8,128)(2,1)S(1)}) custom-call(bf16[256,256]{1,0:T(8,128)(2,1)S(1)} %copy-done.5, bf16[256,256]{1,0:T(8,128)(2,1)S(1)} %copy-done.6, bf16[256,256]{1,0:T(8,128)(2,1)S(1)} %copy-done.7, ...), custom_call_target="tpu_custom_call" | custom-call | flops 268435456 | bytes 3109920 | tf_op jit(solution)/shard_map/pallas_call | solution.py:78
  128.7 3.4 %collective-permute-start.5 = (bf16[4,256,128]{2,1,0:T(8,128)(2,1)S(1)}, bf16[4,256,128]{2,1,0:T(8,128)(2,1)S(1)}, u32[]{:S(2)}, u32[]{:S(2)}) collective-permute-start(bf16[4,256,128]{2,1,0:T(8,128)(2,1)S(1)} %get-tuple-element.32), channel_id=1, source_target_pairs={{0,1},{1,2},{2,3},{3,0},{4,5},{5,6},{6,7},{7,4},{8,9},{9,10},{10,1... | collective-permute-start | bytes 786440 | tf_op jit(solution)/shard_map/ppermute | solution.py:506
  132.1 2.7 %collective-permute-start.6 = (bf16[4,256,128]{2,1,0:T(8,128)(2,1)S(1)}, bf16[4,256,128]{2,1,0:T(8,128)(2,1)S(1)}, u32[]{:S(2)}, u32[]{:S(2)}) collective-permute-start(bf16[4,256,128]{2,1,0:T(8,128)(2,1)S(1)} %get-tuple-element.33), channel_id=1, source_target_pairs={{0,2},{1,3},{2,0},{3,1},{4,6},{5,7},{6,4},{7,5},{8,10},{9,11},{10,... | collective-permute-start | bytes 786440 | tf_op jit(solution)/shard_map/ppermute | solution.py:506
  134.8 4.3 %collective-permute-start.7 = (bf16[4,256,128]{2,1,0:T(8,128)(2,1)S(1)}, bf16[4,256,128]{2,1,0:T(8,128)(2,1)S(1)}, u32[]{:S(2)}, u32[]{:S(2)}) collective-permute-start(bf16[4,256,128]{2,1,0:T(8,128)(2,1)S(1)} %get-tuple-element.34), channel_id=1, source_target_pairs={{0,3},{1,0},{2,1},{3,2},{4,7},{5,4},{6,5},{7,6},{8,11},{9,8},{10,9... | collective-permute-start | bytes 786440 | tf_op jit(solution)/shard_map/ppermute | solution.py:506
  139.8 5.0 %collective-permute-done.6.refs_2_ = bf16[4,256,128]{2,1,0:T(8,128)(2,1)S(1)} collective-permute-done((bf16[4,256,128]{2,1,0:T(8,128)(2,1)S(1)}, bf16[4,256,128]{2,1,0:T(8,128)(2,1)S(1)}, u32[]{:S(2)}, u32[]{:S(2)}) %collective-permute-start.6) | collective-permute-done | bytes 262176 | tf_op jit(solution)/shard_map/ppermute | solution.py:506
  144.7 4.0 %collective-permute-done.7.refs_3_ = bf16[4,256,128]{2,1,0:T(8,128)(2,1)S(1)} collective-permute-done((bf16[4,256,128]{2,1,0:T(8,128)(2,1)S(1)}, bf16[4,256,128]{2,1,0:T(8,128)(2,1)S(1)}, u32[]{:S(2)}, u32[]{:S(2)}) %collective-permute-start.7) | collective-permute-done | bytes 262176 | tf_op jit(solution)/shard_map/ppermute | solution.py:506
  148.9 3.4 %collective-permute-start.8 = (bf16[256,128]{1,0:T(8,128)(2,1)S(1)}, bf16[256,128]{1,0:T(8,128)(2,1)S(1)}, u32[]{:S(2)}, u32[]{:S(2)}) collective-permute-start(bf16[256,128]{1,0:T(8,128)(2,1)S(1)} %get-tuple-element.36), channel_id=1, source_target_pairs={{0,4},{1,5},{2,6},{3,7},{4,8},{5,9},{6,10},{7,11},{8,12},{9,13},{1... | collective-permute-start | bytes 196616 | tf_op jit(solution)/shard_map/ppermute | solution.py:506
  152.3 4.6 %collective-permute-start.9 = (bf16[256,128]{1,0:T(8,128)(2,1)S(1)}, bf16[256,128]{1,0:T(8,128)(2,1)S(1)}, u32[]{:S(2)}, u32[]{:S(2)}) collective-permute-start(bf16[256,128]{1,0:T(8,128)(2,1)S(1)} %get-tuple-element.37), channel_id=1, source_target_pairs={{0,8},{1,9},{2,10},{3,11},{4,12},{5,13},{6,14},{7,15},{8,0},{9,1},... | collective-permute-start | bytes 196616 | tf_op jit(solution)/shard_map/ppermute | solution.py:506
  156.9 3.4 %collective-permute-start.10 = (bf16[256,128]{1,0:T(8,128)(2,1)S(1)}, bf16[256,128]{1,0:T(8,128)(2,1)S(1)}, u32[]{:S(2)}, u32[]{:S(2)}) collective-permute-start(bf16[256,128]{1,0:T(8,128)(2,1)S(1)} %get-tuple-element.38), channel_id=1, source_target_pairs={{0,12},{1,13},{2,14},{3,15},{4,0},{5,1},{6,2},{7,3},{8,4},{9,5},{1... | collective-permute-start | bytes 196616 | tf_op jit(solution)/shard_map/ppermute | solution.py:506
  160.3 2.8 %collective-permute-done.10.refs_3_ = bf16[256,128]{1,0:T(8,128)(2,1)S(1)} collective-permute-done((bf16[256,128]{1,0:T(8,128)(2,1)S(1)}, bf16[256,128]{1,0:T(8,128)(2,1)S(1)}, u32[]{:S(2)}, u32[]{:S(2)}) %collective-permute-start.10) | collective-permute-done | bytes 65568 | tf_op jit(solution)/shard_map/ppermute | solution.py:506
  (54 shorter events, 9.8 us)
Async XLA Ops:
  54.5 27.5 %all-to-all-start.2 = ((bf16[16,320,128]{2,1,0:T(8,128)(2,1)}), bf16[16,320,128]{2,1,0:T(8,128)(2,1)S(1)}, u32[]{:S(2)}, u32[]{:S(2)}) async-start(bf16[16,320,128]{2,1,0:T(8,128)(2,1)} %shard_map.213), calls=%async_computation.2 | async-start | bytes 2621440 | tf_op jit(solution)/shard_map/all_to_all | solution.py:376
  59.4 6.2 %collective-permute-start = (bf16[24,256]{1,0:T(8,128)(2,1)S(1)}, bf16[24,256]{1,0:T(8,128)(2,1)S(1)}, u32[]{:S(2)}, u32[]{:S(2)}) collective-permute-start(bf16[24,256]{1,0:T(8,128)(2,1)S(1)} %copy-done.17), channel_id=1, source_target_pairs={{0,16},{16,32},{32,48},{48,64},{64,80},{80,96},{96,112},{112,128},... | collective-permute-start | bytes 36872 | tf_op jit(solution)/shard_map/ppermute | solution.py:424
  72.1 54.4 %copy-start = (bf16[256,2048]{1,0:T(8,128)(2,1)S(1)}, bf16[256,2048]{1,0:T(8,128)(2,1)}, u32[]{:S(2)}) copy-start(bf16[256,2048]{1,0:T(8,128)(2,1)} %weight_ref.1) | copy-start | bytes 3145732
  72.1 54.4 %copy-start.4 = (bf16[256,256]{1,0:T(8,128)(2,1)S(1)}, bf16[256,256]{1,0:T(8,128)(2,1)}, u32[]{:S(2)}) copy-start(bf16[256,256]{1,0:T(8,128)(2,1)} %gate_ref.1) | copy-start | bytes 393220
  72.1 54.4 %copy-start.5 = (bf16[256,256]{1,0:T(8,128)(2,1)S(1)}, bf16[256,256]{1,0:T(8,128)(2,1)}, u32[]{:S(2)}) copy-start(bf16[256,256]{1,0:T(8,128)(2,1)} %get-tuple-element.22.x_ref) | copy-start | bytes 393220
  72.1 54.4 %copy-start.6 = (bf16[256,256]{1,0:T(8,128)(2,1)S(1)}, bf16[256,256]{1,0:T(8,128)(2,1)}, u32[]{:S(2)}) copy-start(bf16[256,256]{1,0:T(8,128)(2,1)} %get-tuple-element.23.b_ref) | copy-start | bytes 393220
  72.1 54.4 %copy-start.7 = (bf16[256,256]{1,0:T(8,128)(2,1)S(1)}, bf16[256,256]{1,0:T(8,128)(2,1)}, u32[]{:S(2)}) copy-start(bf16[256,256]{1,0:T(8,128)(2,1)} %get-tuple-element.24.c_ref) | copy-start | bytes 393220
  72.1 54.4 %copy-start.8 = (f32[256,128]{1,0:T(8,128)S(1)}, f32[256,128]{1,0:T(8,128)}, u32[]{:S(2)}) copy-start(f32[256,128]{1,0:T(8,128)} %get-tuple-element.25.first_ref) | copy-start | bytes 393220
  72.1 54.4 %copy-start.9 = (f32[256,4]{0,1:T(4,128)S(1)}, f32[256,4]{0,1:T(4,128)}, u32[]{:S(2)}) copy-start(f32[256,4]{0,1:T(4,128)} %param.24) | copy-start | bytes 12292
  72.2 54.4 %copy-start.10 = (f32[256,4]{0,1:T(4,128)S(1)}, f32[256,4]{0,1:T(4,128)}, u32[]{:S(2)}) copy-start(f32[256,4]{0,1:T(4,128)} %param.25) | copy-start | bytes 12292
  72.2 54.4 %copy-start.12 = (f32[4]{0:T(128)S(1)}, f32[4]{0:T(128)}, u32[]{:S(2)}) copy-start(f32[4]{0:T(128)} %param.29) | copy-start | bytes 52
  72.2 54.4 %copy-start.13 = (f32[256]{0:T(256)S(1)}, f32[256]{0:T(256)}, u32[]{:S(2)}) copy-start(f32[256]{0:T(256)} %param.31) | copy-start | bytes 3076
  72.2 54.4 %copy-start.15 = (f32[4]{0:T(128)S(1)}, f32[4]{0:T(128)}, u32[]{:S(2)}) copy-start(f32[4]{0:T(128)} %param.30) | copy-start | bytes 52
  72.3 7.5 %collective-permute-start.1 = (bf16[272,128]{1,0:T(8,128)(2,1)S(1)}, bf16[272,128]{1,0:T(8,128)(2,1)S(1)}, u32[]{:S(2)}, u32[]{:S(2)}) collective-permute-start(bf16[272,128]{1,0:T(8,128)(2,1)S(1)} %shard_map.205.own_ref), channel_id=1, source_target_pairs={{0,32},{32,64},{64,96},{96,128},{128,160},{160,192},{192,224},{224... | collective-permute-start | bytes 208904 | tf_op jit(solution)/shard_map/ppermute | solution.py:448
  80.0 14.0 %collective-permute-start.2 = (bf16[272,128]{1,0:T(8,128)(2,1)S(1)}, bf16[272,128]{1,0:T(8,128)(2,1)S(1)}, u32[]{:S(2)}, u32[]{:S(2)}) collective-permute-start(bf16[272,128]{1,0:T(8,128)(2,1)S(1)} %shard_map.206.own_ref), channel_id=1, source_target_pairs={{0,64},{32,96},{64,128},{96,160},{128,192},{160,224},{192,256},{22... | collective-permute-start | bytes 208904 | tf_op jit(solution)/shard_map/ppermute | solution.py:448
  83.0 80.7 %all-to-all-start.3 = ((bf16[32,16,128]{2,1,0:T(8,128)(2,1)}), bf16[32,16,128]{2,1,0:T(8,128)(2,1)S(1)}, u32[]{:S(2)}, u32[]{:S(2)}) async-start(bf16[32,16,128]{2,1,0:T(8,128)(2,1)} %bitcast.13), calls=%async_computation.3 | async-start | bytes 262144 | tf_op jit(solution)/shard_map/all_to_all | solution.py:376
  94.2 16.5 %collective-permute-start.3 = (bf16[272,128]{1,0:T(8,128)(2,1)S(1)}, bf16[272,128]{1,0:T(8,128)(2,1)S(1)}, u32[]{:S(2)}, u32[]{:S(2)}) collective-permute-start(bf16[272,128]{1,0:T(8,128)(2,1)S(1)} %get-tuple-element.27.own_ref), channel_id=1, source_target_pairs={{0,128},{32,160},{64,192},{96,224},{128,256},{160,288},{192,320},{... | collective-permute-start | bytes 208904 | tf_op jit(solution)/shard_map/ppermute | solution.py:448
  110.8 15.8 %collective-permute-start.4 = (bf16[272,128]{1,0:T(8,128)(2,1)S(1)}, bf16[272,128]{1,0:T(8,128)(2,1)S(1)}, u32[]{:S(2)}, u32[]{:S(2)}) collective-permute-start(bf16[272,128]{1,0:T(8,128)(2,1)S(1)} %get-tuple-element.29), channel_id=1, source_target_pairs={{0,256},{32,288},{64,320},{96,352},{128,384},{160,416},{192,448},{... | collective-permute-start | bytes 208904 | tf_op jit(solution)/shard_map/ppermute | solution.py:448
  128.7 11.0 %collective-permute-start.5 = (bf16[4,256,128]{2,1,0:T(8,128)(2,1)S(1)}, bf16[4,256,128]{2,1,0:T(8,128)(2,1)S(1)}, u32[]{:S(2)}, u32[]{:S(2)}) collective-permute-start(bf16[4,256,128]{2,1,0:T(8,128)(2,1)S(1)} %get-tuple-element.32), channel_id=1, source_target_pairs={{0,1},{1,2},{2,3},{3,0},{4,5},{5,6},{6,7},{7,4},{8,9},{9,10},{10,1... | collective-permute-start | bytes 786440 | tf_op jit(solution)/shard_map/ppermute | solution.py:506
  132.1 12.6 %collective-permute-start.6 = (bf16[4,256,128]{2,1,0:T(8,128)(2,1)S(1)}, bf16[4,256,128]{2,1,0:T(8,128)(2,1)S(1)}, u32[]{:S(2)}, u32[]{:S(2)}) collective-permute-start(bf16[4,256,128]{2,1,0:T(8,128)(2,1)S(1)} %get-tuple-element.33), channel_id=1, source_target_pairs={{0,2},{1,3},{2,0},{3,1},{4,6},{5,7},{6,4},{7,5},{8,10},{9,11},{10,... | collective-permute-start | bytes 786440 | tf_op jit(solution)/shard_map/ppermute | solution.py:506
  134.8 13.9 %collective-permute-start.7 = (bf16[4,256,128]{2,1,0:T(8,128)(2,1)S(1)}, bf16[4,256,128]{2,1,0:T(8,128)(2,1)S(1)}, u32[]{:S(2)}, u32[]{:S(2)}) collective-permute-start(bf16[4,256,128]{2,1,0:T(8,128)(2,1)S(1)} %get-tuple-element.34), channel_id=1, source_target_pairs={{0,3},{1,0},{2,1},{3,2},{4,7},{5,4},{6,5},{7,6},{8,11},{9,8},{10,9... | collective-permute-start | bytes 786440 | tf_op jit(solution)/shard_map/ppermute | solution.py:506
  148.9 11.4 %collective-permute-start.8 = (bf16[256,128]{1,0:T(8,128)(2,1)S(1)}, bf16[256,128]{1,0:T(8,128)(2,1)S(1)}, u32[]{:S(2)}, u32[]{:S(2)}) collective-permute-start(bf16[256,128]{1,0:T(8,128)(2,1)S(1)} %get-tuple-element.36), channel_id=1, source_target_pairs={{0,4},{1,5},{2,6},{3,7},{4,8},{5,9},{6,10},{7,11},{8,12},{9,13},{1... | collective-permute-start | bytes 196616 | tf_op jit(solution)/shard_map/ppermute | solution.py:506
  152.3 8.0 %collective-permute-start.9 = (bf16[256,128]{1,0:T(8,128)(2,1)S(1)}, bf16[256,128]{1,0:T(8,128)(2,1)S(1)}, u32[]{:S(2)}, u32[]{:S(2)}) collective-permute-start(bf16[256,128]{1,0:T(8,128)(2,1)S(1)} %get-tuple-element.37), channel_id=1, source_target_pairs={{0,8},{1,9},{2,10},{3,11},{4,12},{5,13},{6,14},{7,15},{8,0},{9,1},... | collective-permute-start | bytes 196616 | tf_op jit(solution)/shard_map/ppermute | solution.py:506
  156.9 6.2 %collective-permute-start.10 = (bf16[256,128]{1,0:T(8,128)(2,1)S(1)}, bf16[256,128]{1,0:T(8,128)(2,1)S(1)}, u32[]{:S(2)}, u32[]{:S(2)}) collective-permute-start(bf16[256,128]{1,0:T(8,128)(2,1)S(1)} %get-tuple-element.38), channel_id=1, source_target_pairs={{0,12},{1,13},{2,14},{3,15},{4,0},{5,1},{6,2},{7,3},{8,4},{9,5},{1... | collective-permute-start | bytes 196616 | tf_op jit(solution)/shard_map/ppermute | solution.py:506
  (7 other events, 158.0 us)

commit v2 on v0

--- a/solution.py
+++ b/solution.py
@@ -1,5 +1,3 @@
-import functools
-
 import jax
 import jax.numpy as jnp
 from jax import lax
@@ -13,7 +11,8 @@
 BLOCK = 128
 CHIPS = "ep_0"
 EP = (CHIPS, "core")
-SLOTS = 16
+LANES = 128
+PACK = 2
 NOTE = 16
 VMEM = 16 << 20
 WHOLE_VMEM = 60 << 20
@@ -94,7 +93,7 @@
     return wide.T[:, : ref.shape[0]]
 
 
-def slots_of(routing_ref):
+def slots_of(routing_ref, experts):
     tokens = routing_ref.shape[1]
     expert = iota((tokens, 128), 1)
     named = upright(routing_ref).astype(jnp.int32)
@@ -102,11 +101,29 @@
     second = expert == named[:, 1:2]
     member = jnp.where(first | second, 1.0, 0.0).astype(BF16)
     earlier = jnp.where(iota((tokens, tokens), 0) > iota((tokens, tokens), 1), 1.0, 0.0)
-    place = dot(earlier.astype(BF16), member) + (expert * SLOTS).astype(F32)
-    return [
-        jnp.sum(jnp.where(chosen, place, 0.0), axis=1, keepdims=True).astype(jnp.int32)
-        for chosen in (first, second)
-    ]
+    place = dot(earlier.astype(BF16), member)
+    slots = []
+    for index, chosen in enumerate((first, second)):
+        rank = jnp.sum(jnp.where(chosen, place, 0.0), axis=1, keepdims=True).astype(jnp.int32)
+        number = named[:, index : index + 1] * PACK + rank % PACK
+        slots.append(rank // PACK * (PACK * experts) + number)
+    return slots
+
+
+def pack_rows(rows, held, out_ref):
+    experts = out_ref.shape[0]
+    span = PACK * experts
+    for k in range(out_ref.shape[2] // LANES):
+        held[:, k * LANES : (k + 1) * LANES] = rows[k * span : (k + 1) * span, :]
+    for e in range(experts):
+        out_ref[e] = held[PACK * e : PACK * (e + 1), :]
+
+
+def unpack_rows(in_ref, held):
+    for e in range(in_ref.shape[0]):
+        held[PACK * e : PACK * (e + 1), :] = in_ref[e]
+    parts = [held[:, k : k + LANES] for k in range(0, in_ref.shape[2], LANES)]
+    return jnp.concatenate(parts, axis=0)
 
 
 def log_decay_of(step_ref, extra_ref, rate_ref):
@@ -115,27 +132,24 @@
 
 
 def dispatch_body(
-    tok_ref, gain_ref, routing_ref, x_ref, b_ref, c_ref, out_ref, edge_ref
+    tok_ref, gain_ref, routing_ref, x_ref, b_ref, c_ref, out_ref, edge_ref, held
 ):
     tokens, model = tok_ref.shape
     rows = tok_ref[...].astype(F32)
     scale = lax.rsqrt(jnp.sum(rows * rows, axis=1, keepdims=True) * (1.0 / model) + eps)
     columns = pl.ds(pl.multiple_of(lax.axis_index("tp") * 128, 128), 128)
     own = (tok_ref[:, columns].astype(F32) * scale * gain_ref[:, columns]).astype(BF16)
-    slots = slots_of(routing_ref)
-    place = iota((tokens, out_ref.shape[0]), 1)
+    experts = out_ref.shape[0]
+    slots = slots_of(routing_ref, experts)
+    place = iota((tokens, out_ref.shape[1] * experts * out_ref.shape[2] // LANES), 1)
     pick = jnp.where((place == slots[0]) | (place == slots[1]), 1.0, 0.0).astype(BF16)
-    out_ref[...] = dot(pick, own, 0, 0).astype(BF16)
+    pack_rows(dot(pick, own, 0, 0).astype(BF16), held, out_ref)
     for k, ref in enumerate((x_ref, b_ref, c_ref)):
         edge_ref[8 * k : 8 * k + 8, :] = ref[...]
 
 
-def spread_body(capacity, in_ref, out_ref):
-    count = out_ref.shape[1]
-    row = iota((count, in_ref.shape[0]), 0)
-    source = row // capacity * SLOTS + row % capacity
-    pick = jnp.where(iota(source.shape, 1) == source, 1.0, 0.0).astype(BF16)
-    packed = dot(pick, in_ref[...]).astype(BF16)
+def spread_body(in_ref, out_ref, held):
+    packed = unpack_rows(in_ref, held)
     for peer in range(out_ref.shape[0]):
         out_ref[peer] = packed
 
@@ -163,28 +177,24 @@
     return total.astype(BF16)
 
 
-def expert_sum_body(capacity, in_ref, out_ref):
-    total = sum_of(in_ref)
-    count = total.shape[0]
-    row = iota((out_ref.shape[0], count), 0)
-    source = jnp.where(row % SLOTS < capacity, row // SLOTS * capacity + row % SLOTS, -1)
-    pick = jnp.where(iota(source.shape, 1) == source, 1.0, 0.0).astype(BF16)
-    out_ref[...] = dot(pick, total).astype(BF16)
+def expert_sum_body(in_ref, out_ref, held):
+    pack_rows(sum_of(in_ref), held, out_ref)
 
 
 def sum_body(in_ref, out_ref):
     out_ref[...] = sum_of(in_ref)
 
 
-def combine_body(table_ref, routing_ref, score_ref, out_ref):
+def combine_body(table_ref, routing_ref, score_ref, out_ref, held):
     tokens = routing_ref.shape[1]
     scores = upright(score_ref)
     whole = scores[:, 0:1] + scores[:, 1:2]
-    place = iota((tokens, table_ref.shape[0]), 1)
+    table = unpack_rows(table_ref, held)
+    place = iota((tokens, table.shape[0]), 1)
     total = jnp.zeros(out_ref.shape, F32)
-    for index, slot in enumerate(slots_of(routing_ref)):
+    for index, slot in enumerate(slots_of(routing_ref, table_ref.shape[0])):
         pick = jnp.where(place == slot, 1.0, 0.0).astype(BF16)
-        total = total + scores[:, index : index + 1] / whole * dot(pick, table_ref[...])
+        total = total + scores[:, index : index + 1] / whole * dot(pick, table)
     out_ref[...] = total.astype(BF16)
 
 
@@ -288,8 +298,17 @@
     write_log(ref, value[1], wide_ref)
 
 
+def read_half(both_ref, k):
+    half = (both_ref.shape[1] - NOTE) // 2
+    core = lax.axis_index("core")
+    state = both_ref[k, pl.ds(pl.multiple_of(core * half, half), half), :].astype(F32)
+    _, log = read(both_ref[k])
+    heads = log.shape[1] // 2
+    return state, jnp.where(core == 0, log[:, :heads], log[:, heads:])
+
+
 def join_core_body(both_ref, out_ref, wide_ref):
-    write(out_ref, joined(read(both_ref[0]), read(both_ref[1])), wide_ref)
+    write(out_ref, joined(read_half(both_ref, 0), read_half(both_ref, 1)), wide_ref)
 
 
 def join_first_body(came_ref, own_ref, out_ref, wide_ref):
@@ -302,17 +321,21 @@
     write(new_ref, joined(came, read(before_ref[...])), wide_ref)
 
 
-def income_of(came_ref, before_ref, both_ref):
-    state = joined(read(came_ref[...]), read(before_ref[...]))
-    inside = joined(state, read(both_ref[0]))
-    return jnp.where(lax.axis_index("core") == 1, inside[0], state[0])
+def join_last_body(came_ref, before_ref, out_ref):
+    out_ref[...] = joined(read(came_ref[...]), read(before_ref[...]))[0]
+
+
+def income_of(chips_ref, both_ref):
+    state = chips_ref[...]
+    inside, _ = joined((state, 0.0), read(both_ref[0]))
+    return jnp.where(lax.axis_index("core") == 1, inside, state)
 
 
 def mixer_body(
-    x_ref, b_ref, c_ref, gate_ref, first_ref, came_ref, before_ref, both_ref, step_ref, extra_ref,
+    x_ref, b_ref, c_ref, gate_ref, first_ref, chips_ref, both_ref, step_ref, extra_ref,
     rate_ref, skip_ref, gain_ref, weight_ref, out_ref, normed, income_ref,
 ):
-    income_ref[...] = income_of(came_ref, before_ref, both_ref)
+    income_ref[...] = income_of(chips_ref, both_ref)
     step_all, log_all = log_decay_of(step_ref, extra_ref, rate_ref)
     wide = (BLOCK, 128)
     causal = iota(wide, 0) >= iota(wide, 1)
@@ -383,26 +406,28 @@
     tokens, model = expert_input_tokens.shape
     top = routing.shape[1]
     capacity = (tokens * top * 5 + 4 * devices - 1) // (4 * devices)
-    slots = devices * SLOTS
+    message = (devices, PACK, capacity // PACK * LANES)
+    folded = pltpu.VMEM((devices * PACK, message[2]), BF16)
+    slots = devices * capacity
     rate, skip = decay_rate_log[None], head_skip_weight[None]
     step_rows, extra_rows = step_size_logits.T, extra_log_decay.T
     routing_rows = routing.T
 
     outgoing, edge = kernel_call(
         dispatch_body,
-        [shape((slots, 128), BF16), shape((24, channels), BF16)],
+        [shape(message, BF16), shape((24, channels), BF16)],
         (
             expert_input_tokens, expert_norm_gain[None], routing_rows,
             mixer_input_channels, input_state_projection, output_state_projection,
         ),
         2 * slots * tokens * 128,
+        [folded],
         far=(0, 1, 2, 3, 4, 5),
         tails=(3, 4, 5),
         vmem=WHOLE_VMEM,
     )
     prior = lax.ppermute(edge, EP, [(i, i + 1) for i in range(devices - 1)])
-    arrived = all_to_all(outgoing.reshape(devices, SLOTS, 128), EP)
-    arrived = arrived.reshape(slots, 128)
+    arrived = all_to_all(outgoing, EP)
 
     note = channels + NOTE
     wide = pltpu.VMEM((NOTE, 128), F32)
@@ -426,8 +451,11 @@
         route = [(i, i + distance) for i in range(chips - distance)]
         return lax.ppermute(value, CHIPS, route)
 
+    half = channels // 2
+    carried = shape((half + NOTE, STATE), BF16)
+
     def join(body, values, more=()):
-        outs = [shape((note, STATE), BF16), *more]
+        outs = [carried, *more]
         return kernel_call(body, outs, values, 4 * channels * STATE, [wide])
 
     both = lax.all_gather(total, "core")
@@ -436,14 +464,18 @@
     (upto,) = join(join_first_body, (came, upto))
     for distance in (2, 4):
         came = moved(upto, distance)
-        upto, before = join(join_body, (came, upto, before), [shape((note, STATE), F32)])
-    came = moved(upto, 8)
+        upto, before = join(join_body, (came, upto, before), [shape(carried.shape, F32)])
+    (chips,) = kernel_call(
+        join_last_body, [shape((half, STATE), F32)], (moved(upto, 8), before), 4 * half * STATE
+    )
+    chips = lax.all_gather(chips, "core", tiled=True)
 
     (copies,) = kernel_call(
-        functools.partial(spread_body, capacity),
+        spread_body,
         [shape((parts, devices * capacity, 128), BF16)],
         (arrived,),
-        2 * slots * devices * capacity * 128,
+        parts * slots * 128,
+        [folded],
     )
     gathered = all_to_all(copies, "tp")
 
@@ -461,7 +493,7 @@
         mixer_body,
         [shape((parts, length, 128), BF16)],
         (
-            x_conv, b_conv, c_conv, output_gate_logits, first, came, before, both,
+            x_conv, b_conv, c_conv, output_gate_logits, first, chips, both,
             step_rows, extra_rows, rate, skip, grouped_norm_gain[None], mixer_output_weight,
         ),
         2 * length * channels * model,
@@ -470,12 +502,9 @@
     mixer_parts = all_to_all(mixer_part, "tp")
 
     (back,) = kernel_call(
-        functools.partial(expert_sum_body, capacity),
-        [shape((slots, 128), BF16)],
-        (expert_parts,),
-        2 * slots * devices * capacity * 128,
-    )
-    table = all_to_all(back.reshape(devices, SLOTS, 128), EP).reshape(slots, 128)
+        expert_sum_body, [shape(message, BF16)], (expert_parts,), parts * slots * 128, [folded]
+    )
+    table = all_to_all(back, EP)
 
     (mixer_output_first,) = kernel_call(
         sum_body, [shape((length, 128), BF16)], (mixer_parts,), parts * length * 128
@@ -485,6 +514,7 @@
         [shape((tokens, 128), BF16)],
         (table, routing_rows, router_chosen_scores.T),
         4 * tokens * slots * 128,
+        [folded],
     )
     return (mixer_output_first, moe_out)
 

time: 178 us -> 174 us (0.978)
  starting transfers between devices: 61.1 us -> 55.7 us
  blocking collectives: 59.5 us -> 62.7 us
  waiting for transfers between devices: 35.2 us -> 33.4 us
    ppermute x4, starting transfers between devices: 30.6 us -> 25.1 us  [moved(): return lax.ppermute(value, CHIPS, route)]
    all_gather x0 -> x1, blocking collectives: none -> 5.37 us  [per_device(): chips = lax.all_gather(chips, 'core', tiled=True)]
    all_to_all x2, blocking collectives: 57.4 us -> 55.2 us  [all_to_all(): return lax.all_to_all(value, axis, split_axis=0, concat_axis=0, tiled=True)]
    pallas_call x12 -> x13, Pallas kernels: 16 us -> 16.3 us  [kernel_call(): pl.pallas_call(body, out_shape=outs, in_specs=specs, out_specs=[pl.BlockS...]
where the time goes in v2:
time: 174 us; the launch traced here: 173 us
  blocking collectives  62.7 us (36%)
  starting transfers between devices  55.7 us (32%)
  waiting for transfers between devices  33.4 us (19%)
  Pallas kernels  16.3 us (9%)
  local copies, waits for them, and re-layouts  4.29 us (2%)
    all_to_all x2, blocking collectives, all_to_all(): return lax.all_to_all(value, axis, split_axis=0, concat_axis=0, tiled=True)  55.2 us
    all_to_all x3, waiting for transfers between devices, all_to_all(): return lax.all_to_all(value, axis, split_axis=0, concat_axis=0, tiled=True)  28.4 us
    all_to_all x3, starting transfers between devices, all_to_all(): return lax.all_to_all(value, axis, split_axis=0, concat_axis=0, tiled=True)  25.3 us
    ppermute x4, starting transfers between devices, moved(): return lax.ppermute(value, CHIPS, route)  25.1 us
    pallas_call x13, Pallas kernels, kernel_call(): pl.pallas_call(body, out_shape=outs, in_specs=specs, out_specs=[pl.BlockS...  16.3 us
    all_gather x1, blocking collectives, per_device(): chips = lax.all_gather(chips, 'core', tiled=True)  5.37 us
    ppermute x1, starting transfers between devices, per_device(): prior = lax.ppermute(edge, EP, [(i, i + 1) for i in range(devices - 1)])  5.22 us
    unnamed x36, local copies, waits for them, and re-layouts  4.29 us
  transfers between devices with their start and end apart: 8, of which 7 were waited for; matrix products, arithmetic and copies ran while one was open for 0% of the time, Pallas kernels for 5%

profile of v2, /device:TPU:1, one launch (start us, length us, event | category | flops | bytes accessed | tf_op | source)
XLA Modules:
  0.0 173.3 jit_solution(8731688140882573776)
XLA Ops:
  0.6 2.6 %shard_map.203 = (bf16[32,2,640]{2,1,0:T(2,128)(2,1)}, bf16[24,256]{1,0:T(8,128)(2,1)}) custom-call(bf16[128,2048]{1,0:T(8,128)(2,1)} %refs_0_.2, f32[1,2048]{1,0:T(1,128)} %bitcast.28, s32[2,128]{1,0:T(2,128)} %bitcast.21, bf16[256,256]{1,0:T(8,128)(2,1)} %refs_0_.3, bf16[256,256]{1,0:T(8,128)(2,1)} %refs_1_.1, bf16[256,256]{1,0:T(8,128)(2,1)} %refs_2_.1), custom_call_target="tpu_custom_call" | custom-call | flops 10485760 | bytes 1020928 | tf_op jit(solution)/shard_map/pallas_call | solution.py:76
  3.2 30.5 %all_to_all.25.in_ref = bf16[32,2,640]{2,1,0:T(2,128)(2,1)S(1)} all-to-all(bf16[32,2,640]{2,1,0:T(2,128)(2,1)} %get-tuple-element.23), channel_id=1, replica_groups=mesh['ep_0'=16,'core'=2,'tp'=16] {'ep_0','core'}, dimensions={0} | all-to-all | bytes 163840 | tf_op jit(solution)/shard_map/all_to_all | solution.py:378
  34.1 24.7 %all_to_all.26.refs_0_ = bf16[16,320,128]{2,1,0:T(8,128)(2,1)S(1)} all-to-all(bf16[16,320,128]{2,1,0:T(8,128)(2,1)S(1)} %shard_map.212), channel_id=1, replica_groups=mesh['ep_0'=16,'core'=2,'tp'=16] {'tp'}, dimensions={0} | all-to-all | bytes 2621440 | tf_op jit(solution)/shard_map/all_to_all | solution.py:378
  58.8 2.8 %shard_map.213 = bf16[16,320,128]{2,1,0:T(8,128)(2,1)} custom-call(bf16[16,320,128]{2,1,0:T(8,128)(2,1)S(1)} %all_to_all.26.refs_0_, bf16[2048,128]{1,0:T(8,128)(2,1)S(1)} %bitcast.14, bf16[2048,128]{1,0:T(8,128)(2,1)S(1)} %bitcast.15, bf16[128,2048]{1,0:T(8,128)(2,1)S(1)} %bitcast.16), custom_call_target="tpu_custom_call" | custom-call | flops 503316480 | bytes 4194304 | tf_op jit(solution)/shard_map/pallas_call | solution.py:76
  61.6 3.7 %all-to-all-start.3 = ((bf16[16,320,128]{2,1,0:T(8,128)(2,1)}), bf16[16,320,128]{2,1,0:T(8,128)(2,1)S(1)}, u32[]{:S(2)}, u32[]{:S(2)}) async-start(bf16[16,320,128]{2,1,0:T(8,128)(2,1)} %shard_map.213), calls=%async_computation.3 | async-start | bytes 2621440 | tf_op jit(solution)/shard_map/all_to_all | solution.py:378
  65.4 5.2 %collective-permute-start = (bf16[24,256]{1,0:T(8,128)(2,1)S(1)}, bf16[24,256]{1,0:T(8,128)(2,1)S(1)}, u32[]{:S(2)}, u32[]{:S(2)}) collective-permute-start(bf16[24,256]{1,0:T(8,128)(2,1)S(1)} %copy-done.17), channel_id=1, source_target_pairs={{0,16},{16,32},{32,48},{48,64},{64,80},{80,96},{96,112},{112,128},... | collective-permute-start | bytes 36872 | tf_op jit(solution)/shard_map/ppermute | solution.py:429
  72.1 3.7 %shard_map.204 = (bf16[256,256]{1,0:T(8,128)(2,1)}, bf16[256,256]{1,0:T(8,128)(2,1)}, bf16[256,256]{1,0:T(8,128)(2,1)}, f32[256,128]{1,0:T(8,128)}, bf16[272,128]{1,0:T(8,128)(2,1)}) custom-call(bf16[256,256]{1,0:T(8,128)(2,1)} %refs_0_.3, bf16[256,256]{1,0:T(8,128)(2,1)} %refs_1_.1, bf16[256,256]{1,0:T(8,128)(2,1)} %refs_2_.1, bf16[24,256]{1,0:T(8,128)(2,1)} %copy-done.16, ...), custom_call_target="tpu_custom_call" | custom-call | flops 16777216 | bytes 1013776 | tf_op jit(solution)/shard_map/pallas_call | solution.py:76
  75.8 2.1 %all-gather = bf16[544,128]{1,0:T(8,128)(2,1)S(1)} all-gather(bf16[272,128]{1,0:T(8,128)(2,1)} %get-tuple-element.18), channel_id=2, replica_groups=mesh['ep_0'=16,'core'=2,'tp'=16] {'core'}, dimensions={0}, use_global_device_ids=true | all-gather | bytes 208896 | tf_op jit(solution)/shard_map/all_gather | solution.py:461
  78.1 4.0 %collective-permute-start.1 = (bf16[144,128]{1,0:T(8,128)(2,1)S(1)}, bf16[144,128]{1,0:T(8,128)(2,1)S(1)}, u32[]{:S(2)}, u32[]{:S(2)}) collective-permute-start(bf16[144,128]{1,0:T(8,128)(2,1)S(1)} %shard_map.205.own_ref), channel_id=1, source_target_pairs={{0,32},{32,64},{64,96},{96,128},{128,160},{160,192},{192,224},{224... | collective-permute-start | bytes 110600 | tf_op jit(solution)/shard_map/ppermute | solution.py:452
  82.1 1.0 collective-permute-done.1.came_ref.before_ref
  83.3 4.4 %collective-permute-start.2 = (bf16[144,128]{1,0:T(8,128)(2,1)S(1)}, bf16[144,128]{1,0:T(8,128)(2,1)S(1)}, u32[]{:S(2)}, u32[]{:S(2)}) collective-permute-start(bf16[144,128]{1,0:T(8,128)(2,1)S(1)} %shard_map.206.own_ref), channel_id=1, source_target_pairs={{0,64},{32,96},{64,128},{96,160},{128,192},{160,224},{192,256},{22... | collective-permute-start | bytes 110600 | tf_op jit(solution)/shard_map/ppermute | solution.py:452
  87.7 1.0 collective-permute-done.2.came_ref
  88.8 8.5 %collective-permute-start.3 = (bf16[144,128]{1,0:T(8,128)(2,1)S(1)}, bf16[144,128]{1,0:T(8,128)(2,1)S(1)}, u32[]{:S(2)}, u32[]{:S(2)}) collective-permute-start(bf16[144,128]{1,0:T(8,128)(2,1)S(1)} %get-tuple-element.19.own_ref), channel_id=1, source_target_pairs={{0,128},{32,160},{64,192},{96,224},{128,256},{160,288},{192,320},{... | collective-permute-start | bytes 110600 | tf_op jit(solution)/shard_map/ppermute | solution.py:452
  97.4 1.0 collective-permute-done.3.came_ref
  98.5 8.3 %collective-permute-start.4 = (bf16[144,128]{1,0:T(8,128)(2,1)S(1)}, bf16[144,128]{1,0:T(8,128)(2,1)S(1)}, u32[]{:S(2)}, u32[]{:S(2)}) collective-permute-start(bf16[144,128]{1,0:T(8,128)(2,1)S(1)} %get-tuple-element.21), channel_id=1, source_target_pairs={{0,256},{32,288},{64,320},{96,352},{128,384},{160,416},{192,448},{... | collective-permute-start | bytes 110600 | tf_op jit(solution)/shard_map/ppermute | solution.py:452
  106.8 1.0 collective-permute-done.4.came_ref
  108.0 5.4 %all_gather.11.chips_ref = f32[256,128]{1,0:T(8,128)S(1)} all-gather(f32[128,128]{1,0:T(8,128)S(1)} %shard_map.209), channel_id=1, replica_groups=mesh['ep_0'=16,'core'=2,'tp'=16] {'core'}, dimensions={0}, use_global_device_ids=true | all-gather | bytes 196608 | tf_op jit(solution)/shard_map/all_gather | solution.py:471
  116.1 0.9 copy-done.8
  117.1 3.1 %shard_map.210 = bf16[16,256,128]{2,1,0:T(8,128)(2,1)} custom-call(bf16[256,256]{1,0:T(8,128)(2,1)S(1)} %copy-done.5, bf16[256,256]{1,0:T(8,128)(2,1)S(1)} %copy-done.6, bf16[256,256]{1,0:T(8,128)(2,1)S(1)} %copy-done.7, bf16[256,256]{1,0:T(8,128)(2,1)S(1)} %copy-done.4, f32[256,128]{1,0:T(8,128)S(1)} %copy-done.8, f32[256,128]{1,0:T(8,128)S(1)} %all_gather.11.chips_ref, ...), custom_call_target="tpu_custom_call" | custom-call | flops 268435456 | bytes 3032096 | tf_op jit(solution)/shard_map/pallas_call | solution.py:76
  120.1 6.9 %all-to-all-start = ((bf16[16,256,128]{2,1,0:T(8,128)(2,1)}), bf16[16,256,128]{2,1,0:T(8,128)(2,1)S(1)}, u32[]{:S(2)}, u32[]{:S(2)}) async-start(bf16[16,256,128]{2,1,0:T(8,128)(2,1)} %shard_map.210), calls=%async_computation | async-start | bytes 2097152 | tf_op jit(solution)/shard_map/all_to_all | solution.py:378
  127.9 15.4 %all-to-all-done.in_ref = bf16[16,256,128]{2,1,0:T(8,128)(2,1)S(1)} async-done(((bf16[16,256,128]{2,1,0:T(8,128)(2,1)}), bf16[16,256,128]{2,1,0:T(8,128)(2,1)S(1)}, u32[]{:S(2)}, u32[]{:S(2)}) %all-to-all-start) | async-done | bytes 1048608 | tf_op jit(solution)/shard_map/all_to_all | solution.py:378
  143.4 14.7 %all-to-all-start.4 = ((bf16[32,2,640]{2,1,0:T(2,128)(2,1)}), bf16[32,2,640]{2,1,0:T(2,128)(2,1)S(1)}, u32[]{:S(2)}, u32[]{:S(2)}) async-start(bf16[32,2,640]{2,1,0:T(2,128)(2,1)} %shard_map.214), calls=%async_computation.4 | async-start | bytes 163840 | tf_op jit(solution)/shard_map/all_to_all | solution.py:378
  158.8 12.9 %all-to-all-done.4.table_ref = bf16[32,2,640]{2,1,0:T(2,128)(2,1)S(1)} async-done(((bf16[32,2,640]{2,1,0:T(2,128)(2,1)}), bf16[32,2,640]{2,1,0:T(2,128)(2,1)S(1)}, u32[]{:S(2)}, u32[]{:S(2)}) %all-to-all-start.4) | async-done | bytes 81952 | tf_op jit(solution)/shard_map/all_to_all | solution.py:378
  171.8 1.5 shard_map.215
  (45 shorter events, 6.9 us)
Async XLA Ops:
  34.0 24.8 %copy-start.1 = (bf16[1,2048,128]{2,1,0:T(8,128)(2,1)S(1)}, bf16[1,2048,128]{2,1,0:T(8,128)(2,1)}, u32[]{:S(2)}) copy-start(bf16[1,2048,128]{2,1,0:T(8,128)(2,1)} %param.37) | copy-start | bytes 1572868
  34.1 24.8 %copy-start.2 = (bf16[1,2048,128]{2,1,0:T(8,128)(2,1)S(1)}, bf16[1,2048,128]{2,1,0:T(8,128)(2,1)}, u32[]{:S(2)}) copy-start(bf16[1,2048,128]{2,1,0:T(8,128)(2,1)} %param.38) | copy-start | bytes 1572868
  34.1 24.8 %copy-start.3 = (bf16[1,128,2048]{2,1,0:T(8,128)(2,1)S(1)}, bf16[1,128,2048]{2,1,0:T(8,128)(2,1)}, u32[]{:S(2)}) copy-start(bf16[1,128,2048]{2,1,0:T(8,128)(2,1)} %param.39) | copy-start | bytes 1572868
  61.6 3.8 %copy-start.17 = (bf16[24,256]{1,0:T(8,128)(2,1)S(1)}, bf16[24,256]{1,0:T(8,128)(2,1)}, u32[]{:S(2)}) copy-start(bf16[24,256]{1,0:T(8,128)(2,1)} %get-tuple-element.13) | copy-start | bytes 36868
  61.6 58.5 %all-to-all-start.3 = ((bf16[16,320,128]{2,1,0:T(8,128)(2,1)}), bf16[16,320,128]{2,1,0:T(8,128)(2,1)S(1)}, u32[]{:S(2)}, u32[]{:S(2)}) async-start(bf16[16,320,128]{2,1,0:T(8,128)(2,1)} %shard_map.213), calls=%async_computation.3 | async-start | bytes 2621440 | tf_op jit(solution)/shard_map/all_to_all | solution.py:378
  65.3 48.0 %copy-start = (bf16[256,2048]{1,0:T(8,128)(2,1)S(1)}, bf16[256,2048]{1,0:T(8,128)(2,1)}, u32[]{:S(2)}) copy-start(bf16[256,2048]{1,0:T(8,128)(2,1)} %weight_ref.1) | copy-start | bytes 3145732
  65.4 48.0 %copy-start.4 = (bf16[256,256]{1,0:T(8,128)(2,1)S(1)}, bf16[256,256]{1,0:T(8,128)(2,1)}, u32[]{:S(2)}) copy-start(bf16[256,256]{1,0:T(8,128)(2,1)} %gate_ref.1) | copy-start | bytes 393220
  65.4 48.0 %copy-start.9 = (f32[256,4]{0,1:T(4,128)S(1)}, f32[256,4]{0,1:T(4,128)}, u32[]{:S(2)}) copy-start(f32[256,4]{0,1:T(4,128)} %param.24) | copy-start | bytes 12292
  65.4 48.0 %copy-start.10 = (f32[256,4]{0,1:T(4,128)S(1)}, f32[256,4]{0,1:T(4,128)}, u32[]{:S(2)}) copy-start(f32[256,4]{0,1:T(4,128)} %param.25) | copy-start | bytes 12292
  65.4 48.0 %copy-start.12 = (f32[4]{0:T(128)S(1)}, f32[4]{0:T(128)}, u32[]{:S(2)}) copy-start(f32[4]{0:T(128)} %param.29) | copy-start | bytes 52
  65.4 48.0 %copy-start.13 = (f32[256]{0:T(256)S(1)}, f32[256]{0:T(256)}, u32[]{:S(2)}) copy-start(f32[256]{0:T(256)} %param.31) | copy-start | bytes 3076
  65.4 48.0 %copy-start.15 = (f32[4]{0:T(128)S(1)}, f32[4]{0:T(128)}, u32[]{:S(2)}) copy-start(f32[4]{0:T(128)} %param.30) | copy-start | bytes 52
  65.4 6.0 %collective-permute-start = (bf16[24,256]{1,0:T(8,128)(2,1)S(1)}, bf16[24,256]{1,0:T(8,128)(2,1)S(1)}, u32[]{:S(2)}, u32[]{:S(2)}) collective-permute-start(bf16[24,256]{1,0:T(8,128)(2,1)S(1)} %copy-done.17), channel_id=1, source_target_pairs={{0,16},{16,32},{32,48},{48,64},{64,80},{80,96},{96,112},{112,128},... | collective-permute-start | bytes 36872 | tf_op jit(solution)/shard_map/ppermute | solution.py:429
  78.1 5.0 %collective-permute-start.1 = (bf16[144,128]{1,0:T(8,128)(2,1)S(1)}, bf16[144,128]{1,0:T(8,128)(2,1)S(1)}, u32[]{:S(2)}, u32[]{:S(2)}) collective-permute-start(bf16[144,128]{1,0:T(8,128)(2,1)S(1)} %shard_map.205.own_ref), channel_id=1, source_target_pairs={{0,32},{32,64},{64,96},{96,128},{128,160},{160,192},{192,224},{224... | collective-permute-start | bytes 110600 | tf_op jit(solution)/shard_map/ppermute | solution.py:452
  83.3 5.4 %collective-permute-start.2 = (bf16[144,128]{1,0:T(8,128)(2,1)S(1)}, bf16[144,128]{1,0:T(8,128)(2,1)S(1)}, u32[]{:S(2)}, u32[]{:S(2)}) collective-permute-start(bf16[144,128]{1,0:T(8,128)(2,1)S(1)} %shard_map.206.own_ref), channel_id=1, source_target_pairs={{0,64},{32,96},{64,128},{96,160},{128,192},{160,224},{192,256},{22... | collective-permute-start | bytes 110600 | tf_op jit(solution)/shard_map/ppermute | solution.py:452
  88.8 9.6 %collective-permute-start.3 = (bf16[144,128]{1,0:T(8,128)(2,1)S(1)}, bf16[144,128]{1,0:T(8,128)(2,1)S(1)}, u32[]{:S(2)}, u32[]{:S(2)}) collective-permute-start(bf16[144,128]{1,0:T(8,128)(2,1)S(1)} %get-tuple-element.19.own_ref), channel_id=1, source_target_pairs={{0,128},{32,160},{64,192},{96,224},{128,256},{160,288},{192,320},{... | collective-permute-start | bytes 110600 | tf_op jit(solution)/shard_map/ppermute | solution.py:452
  98.5 9.3 %collective-permute-start.4 = (bf16[144,128]{1,0:T(8,128)(2,1)S(1)}, bf16[144,128]{1,0:T(8,128)(2,1)S(1)}, u32[]{:S(2)}, u32[]{:S(2)}) collective-permute-start(bf16[144,128]{1,0:T(8,128)(2,1)S(1)} %get-tuple-element.21), channel_id=1, source_target_pairs={{0,256},{32,288},{64,320},{96,352},{128,384},{160,416},{192,448},{... | collective-permute-start | bytes 110600 | tf_op jit(solution)/shard_map/ppermute | solution.py:452
  113.4 0.9 copy-start.5
  114.3 0.9 copy-start.6
  115.2 0.9 copy-start.7
  120.1 23.2 %all-to-all-start = ((bf16[16,256,128]{2,1,0:T(8,128)(2,1)}), bf16[16,256,128]{2,1,0:T(8,128)(2,1)S(1)}, u32[]{:S(2)}, u32[]{:S(2)}) async-start(bf16[16,256,128]{2,1,0:T(8,128)(2,1)} %shard_map.210), calls=%async_computation | async-start | bytes 2097152 | tf_op jit(solution)/shard_map/all_to_all | solution.py:378
  127.0 44.8 %copy-start.11 = (s32[128,2]{0,1:T(2,128)S(1)}, s32[128,2]{0,1:T(2,128)}, u32[]{:S(2)}) copy-start(s32[128,2]{0,1:T(2,128)} %param.34) | copy-start | bytes 3076
  127.0 44.8 %copy-start.14 = (f32[128,2]{0,1:T(2,128)S(1)}, f32[128,2]{0,1:T(2,128)}, u32[]{:S(2)}) copy-start(f32[128,2]{0,1:T(2,128)} %param.35) | copy-start | bytes 3076
  143.4 28.4 %all-to-all-start.4 = ((bf16[32,2,640]{2,1,0:T(2,128)(2,1)}), bf16[32,2,640]{2,1,0:T(2,128)(2,1)S(1)}, u32[]{:S(2)}, u32[]{:S(2)}) async-start(bf16[32,2,640]{2,1,0:T(2,128)(2,1)} %shard_map.214), calls=%async_computation.4 | async-start | bytes 163840 | tf_op jit(solution)/shard_map/all_to_all | solution.py:378
  (2 other events, 1.5 us)

commit v3 on v2

--- a/solution.py
+++ b/solution.py
@@ -9,8 +9,8 @@
 HEAD_DIM = 64
 STATE = 128
 BLOCK = 128
-CHIPS = "ep_0"
-EP = (CHIPS, "core")
+CHIPS = ("ep_hi", "ep_lo")
+EP = (*CHIPS, "core")
 LANES = 128
 PACK = 2
 NOTE = 16
@@ -321,8 +321,13 @@
     write(new_ref, joined(came, read(before_ref[...])), wide_ref)
 
 
-def join_last_body(came_ref, before_ref, out_ref):
-    out_ref[...] = joined(read(came_ref[...]), read(before_ref[...]))[0]
+def join_far_body(far_ref, before_ref, out_ref):
+    rows = far_ref.shape[1] - NOTE
+    me = lax.axis_index(CHIPS[0])
+    state = jnp.zeros((rows, 128), F32)
+    for k in range(far_ref.shape[0] - 1):
+        state = jnp.where(k < me, joined((state, 0.0), read(far_ref[k]))[0], state)
+    out_ref[...] = joined((state, 0.0), read(before_ref[...]))[0]
 
 
 def income_of(chips_ref, both_ref):
@@ -462,11 +467,10 @@
     (upto,) = join(join_core_body, (both,))
     before = came = moved(upto, 1)
     (upto,) = join(join_first_body, (came, upto))
-    for distance in (2, 4):
-        came = moved(upto, distance)
-        upto, before = join(join_body, (came, upto, before), [shape(carried.shape, F32)])
+    upto, before = join(join_body, (moved(upto, 2), upto, before), [shape(carried.shape, F32)])
+    far = lax.all_gather(upto, CHIPS[0])
     (chips,) = kernel_call(
-        join_last_body, [shape((half, STATE), F32)], (moved(upto, 8), before), 4 * half * STATE
+        join_far_body, [shape((half, STATE), F32)], (far, before), 8 * half * STATE
     )
     chips = lax.all_gather(chips, "core", tiled=True)
 
@@ -520,7 +524,7 @@
 
 
 def solution(mesh):
-    split = Mesh(mesh.devices.reshape(16, 2, mesh.shape["tp"]), (*EP, "tp"))
+    split = Mesh(mesh.devices.reshape(4, 4, 2, mesh.shape["tp"]), (*EP, "tp"))
     in_specs = (
         P(EP, "tp"),
         P(EP, "tp"),

time: 174 us -> 164 us (0.943)
  starting transfers between devices: 55.7 us -> 33.1 us
  blocking collectives: 62.7 us -> 81.1 us
  local copies, waits for them, and re-layouts: 4.29 us -> 0.7 us
  waiting for transfers between devices: 33.4 us -> 31.3 us
    all_gather x0 -> x1, blocking collectives: none -> 17.7 us  [per_device(): far = lax.all_gather(upto, CHIPS[0])]
    ppermute x4 -> x2, starting transfers between devices: 25.1 us -> 8.33 us  [moved(): return lax.ppermute(value, CHIPS, route)]
    all_to_all x3, starting transfers between devices: 25.3 us -> 19.5 us  [all_to_all(): return lax.all_to_all(value, axis, split_axis=0, concat_axis=0, tiled=True)]
    unnamed x36, local copies, waits for them, and re-layouts: 4.29 us -> 0.7 us
    ppermute x4 -> x2, waiting for transfers between devices: 4.17 us -> 2.09 us  [moved(): return lax.ppermute(value, CHIPS, route)]
    pallas_call x13 -> x12, Pallas kernels: 16.3 us -> 16.2 us  [kernel_call(): pl.pallas_call(body, out_shape=outs, in_specs=specs, out_specs=[pl.BlockS...]
  transfers between devices with their start and end apart: 8 -> 6, of which waited for: 7 -> 5; matrix products, arithmetic and copies ran while one was open for 0% -> 0% of each run, Pallas kernels for 5% -> 6%
where the time goes in v3:
time: 164 us; the launch traced here: 163 us
  blocking collectives  81.1 us (49%)
  starting transfers between devices  33.1 us (20%)
  waiting for transfers between devices  31.3 us (19%)
  Pallas kernels  16.2 us (10%)
    all_to_all x2, blocking collectives, all_to_all(): return lax.all_to_all(value, axis, split_axis=0, concat_axis=0, tiled=True)  55.2 us
    all_to_all x3, waiting for transfers between devices, all_to_all(): return lax.all_to_all(value, axis, split_axis=0, concat_axis=0, tiled=True)  28.4 us
    all_to_all x3, starting transfers between devices, all_to_all(): return lax.all_to_all(value, axis, split_axis=0, concat_axis=0, tiled=True)  19.5 us
    all_gather x1, blocking collectives, per_device(): far = lax.all_gather(upto, CHIPS[0])  17.7 us
    pallas_call x12, Pallas kernels, kernel_call(): pl.pallas_call(body, out_shape=outs, in_specs=specs, out_specs=[pl.BlockS...  16.2 us
    ppermute x2, starting transfers between devices, moved(): return lax.ppermute(value, CHIPS, route)  8.33 us
    all_gather x1, blocking collectives, per_device(): chips = lax.all_gather(chips, 'core', tiled=True)  6 us
    ppermute x1, starting transfers between devices, per_device(): prior = lax.ppermute(edge, EP, [(i, i + 1) for i in range(devices - 1)])  5.22 us
  transfers between devices with their start and end apart: 6, of which 5 were waited for; matrix products, arithmetic and copies ran while one was open for 0% of the time, Pallas kernels for 6%

profile of v3, /device:TPU:1, one launch (start us, length us, event | category | flops | bytes accessed | tf_op | source)
XLA Modules:
  0.0 163.3 jit_solution(55324356662633454)
XLA Ops:
  0.6 2.6 %shard_map.203 = (bf16[32,2,640]{2,1,0:T(2,128)(2,1)}, bf16[24,256]{1,0:T(8,128)(2,1)}) custom-call(bf16[128,2048]{1,0:T(8,128)(2,1)} %refs_0_.2, f32[1,2048]{1,0:T(1,128)} %bitcast.30, s32[2,128]{1,0:T(2,128)} %bitcast.23, bf16[256,256]{1,0:T(8,128)(2,1)} %refs_0_.3, bf16[256,256]{1,0:T(8,128)(2,1)} %refs_1_.1, bf16[256,256]{1,0:T(8,128)(2,1)} %refs_2_.1), custom_call_target="tpu_custom_call" | custom-call | flops 10485760 | bytes 1020928 | tf_op jit(solution)/shard_map/pallas_call | solution.py:76
  3.2 30.5 %all_to_all.25.in_ref = bf16[32,2,640]{2,1,0:T(2,128)(2,1)S(1)} all-to-all(bf16[32,2,640]{2,1,0:T(2,128)(2,1)} %get-tuple-element.19), channel_id=1, replica_groups=mesh['ep_hi'=4,'ep_lo'=4,'core'=2,'tp'=16] {'ep_hi','ep_lo','core'}, dimensions={0} | all-to-all | bytes 163840 | tf_op jit(solution)/shard_map/all_to_all | solution.py:383
  34.1 24.7 %all_to_all.26.refs_0_ = bf16[16,320,128]{2,1,0:T(8,128)(2,1)S(1)} all-to-all(bf16[16,320,128]{2,1,0:T(8,128)(2,1)S(1)} %shard_map.211), channel_id=1, replica_groups=mesh['ep_hi'=4,'ep_lo'=4,'core'=2,'tp'=16] {'tp'}, dimensions={0} | all-to-all | bytes 2621440 | tf_op jit(solution)/shard_map/all_to_all | solution.py:383
  58.8 2.8 %shard_map.212 = bf16[16,320,128]{2,1,0:T(8,128)(2,1)} custom-call(bf16[16,320,128]{2,1,0:T(8,128)(2,1)S(1)} %all_to_all.26.refs_0_, bf16[2048,128]{1,0:T(8,128)(2,1)S(1)} %bitcast.16, bf16[2048,128]{1,0:T(8,128)(2,1)S(1)} %bitcast.17, bf16[128,2048]{1,0:T(8,128)(2,1)S(1)} %bitcast.18), custom_call_target="tpu_custom_call" | custom-call | flops 503316480 | bytes 4194304 | tf_op jit(solution)/shard_map/pallas_call | solution.py:76
  61.6 3.7 %all-to-all-start.3 = ((bf16[16,320,128]{2,1,0:T(8,128)(2,1)}), bf16[16,320,128]{2,1,0:T(8,128)(2,1)S(1)}, u32[]{:S(2)}, u32[]{:S(2)}) async-start(bf16[16,320,128]{2,1,0:T(8,128)(2,1)} %shard_map.212), calls=%async_computation.3 | async-start | bytes 2621440 | tf_op jit(solution)/shard_map/all_to_all | solution.py:383
  65.4 5.2 %collective-permute-start = (bf16[24,256]{1,0:T(8,128)(2,1)S(1)}, bf16[24,256]{1,0:T(8,128)(2,1)S(1)}, u32[]{:S(2)}, u32[]{:S(2)}) collective-permute-start(bf16[24,256]{1,0:T(8,128)(2,1)S(1)} %copy-done.17), channel_id=1, source_target_pairs={{0,16},{16,32},{32,48},{48,64},{64,80},{80,96},{96,112},{112,128},... | collective-permute-start | bytes 36872 | tf_op jit(solution)/shard_map/ppermute | solution.py:434
  70.7 0.8 collective-permute-done.refs_3_
  71.5 0.6 copy-done.16
  72.1 3.8 %shard_map.204 = (bf16[256,256]{1,0:T(8,128)(2,1)}, bf16[256,256]{1,0:T(8,128)(2,1)}, bf16[256,256]{1,0:T(8,128)(2,1)}, f32[256,128]{1,0:T(8,128)}, bf16[272,128]{1,0:T(8,128)(2,1)}) custom-call(bf16[256,256]{1,0:T(8,128)(2,1)} %refs_0_.3, bf16[256,256]{1,0:T(8,128)(2,1)} %refs_1_.1, bf16[256,256]{1,0:T(8,128)(2,1)} %refs_2_.1, bf16[24,256]{1,0:T(8,128)(2,1)} %copy-done.16, ...), custom_call_target="tpu_custom_call" | custom-call | flops 16777216 | bytes 1013776 | tf_op jit(solution)/shard_map/pallas_call | solution.py:76
  75.9 2.2 %all-gather = bf16[544,128]{1,0:T(8,128)(2,1)S(1)} all-gather(bf16[272,128]{1,0:T(8,128)(2,1)} %get-tuple-element.16), channel_id=2, replica_groups=mesh['ep_hi'=4,'ep_lo'=4,'core'=2,'tp'=16] {'core'}, dimensions={0}, use_global_device_ids=true | all-gather | bytes 208896 | tf_op jit(solution)/shard_map/all_gather | solution.py:466
  78.3 4.0 %collective-permute-start.1 = (bf16[144,128]{1,0:T(8,128)(2,1)S(1)}, bf16[144,128]{1,0:T(8,128)(2,1)S(1)}, u32[]{:S(2)}, u32[]{:S(2)}) collective-permute-start(bf16[144,128]{1,0:T(8,128)(2,1)S(1)} %shard_map.205.own_ref), channel_id=1, source_target_pairs={{0,32},{32,64},{64,96},{96,128},{128,160},{160,192},{192,224},{224... | collective-permute-start | bytes 110600 | tf_op jit(solution)/shard_map/ppermute | solution.py:457
  82.3 1.0 collective-permute-done.1.came_ref.before_ref
  83.5 4.4 %collective-permute-start.2 = (bf16[144,128]{1,0:T(8,128)(2,1)S(1)}, bf16[144,128]{1,0:T(8,128)(2,1)S(1)}, u32[]{:S(2)}, u32[]{:S(2)}) collective-permute-start(bf16[144,128]{1,0:T(8,128)(2,1)S(1)} %shard_map.206.own_ref), channel_id=1, source_target_pairs={{0,64},{32,96},{64,128},{96,160},{128,192},{160,224},{192,256},{22... | collective-permute-start | bytes 110600 | tf_op jit(solution)/shard_map/ppermute | solution.py:457
  87.8 1.0 collective-permute-done.2.came_ref
  89.0 17.7 %all-gather.1 = bf16[576,128]{1,0:T(8,128)(2,1)S(1)} all-gather(bf16[144,128]{1,0:T(8,128)(2,1)S(1)} %get-tuple-element.17), channel_id=3, replica_groups=mesh['ep_hi'=4,'ep_lo'=4,'core'=2,'tp'=16] {'ep_hi'}, dimensions={0}, use_global_device_ids=true | all-gather | bytes 184320 | tf_op jit(solution)/shard_map/all_gather | solution.py:471
  106.8 6.0 %all_gather.19.chips_ref = f32[256,128]{1,0:T(8,128)S(1)} all-gather(f32[128,128]{1,0:T(8,128)S(1)} %shard_map.208), channel_id=1, replica_groups=mesh['ep_hi'=4,'ep_lo'=4,'core'=2,'tp'=16] {'core'}, dimensions={0}, use_global_device_ids=true | all-gather | bytes 196608 | tf_op jit(solution)/shard_map/all_gather | solution.py:475
  112.9 3.0 %shard_map.209 = bf16[16,256,128]{2,1,0:T(8,128)(2,1)} custom-call(bf16[256,256]{1,0:T(8,128)(2,1)S(1)} %copy-done.5, bf16[256,256]{1,0:T(8,128)(2,1)S(1)} %copy-done.6, bf16[256,256]{1,0:T(8,128)(2,1)S(1)} %copy-done.7, bf16[256,256]{1,0:T(8,128)(2,1)S(1)} %copy-done.4, f32[256,128]{1,0:T(8,128)S(1)} %copy-done.8, f32[256,128]{1,0:T(8,128)S(1)} %all_gather.19.chips_ref, ...), custom_call_target="tpu_custom_call" | custom-call | flops 268435456 | bytes 3032096 | tf_op jit(solution)/shard_map/pallas_call | solution.py:76
  115.9 6.9 %all-to-all-start = ((bf16[16,256,128]{2,1,0:T(8,128)(2,1)}), bf16[16,256,128]{2,1,0:T(8,128)(2,1)S(1)}, u32[]{:S(2)}, u32[]{:S(2)}) async-start(bf16[16,256,128]{2,1,0:T(8,128)(2,1)} %shard_map.209), calls=%async_computation | async-start | bytes 2097152 | tf_op jit(solution)/shard_map/all_to_all | solution.py:383
  122.9 0.9 shard_map.213
  123.7 15.4 %all-to-all-done.in_ref = bf16[16,256,128]{2,1,0:T(8,128)(2,1)S(1)} async-done(((bf16[16,256,128]{2,1,0:T(8,128)(2,1)}), bf16[16,256,128]{2,1,0:T(8,128)(2,1)S(1)}, u32[]{:S(2)}, u32[]{:S(2)}) %all-to-all-start) | async-done | bytes 1048608 | tf_op jit(solution)/shard_map/all_to_all | solution.py:383
  139.2 8.9 %all-to-all-start.4 = ((bf16[32,2,640]{2,1,0:T(2,128)(2,1)}), bf16[32,2,640]{2,1,0:T(2,128)(2,1)S(1)}, u32[]{:S(2)}, u32[]{:S(2)}) async-start(bf16[32,2,640]{2,1,0:T(2,128)(2,1)} %shard_map.213), calls=%async_computation.4 | async-start | bytes 163840 | tf_op jit(solution)/shard_map/all_to_all | solution.py:383
  148.1 0.8 shard_map.210
  148.9 12.9 %all-to-all-done.4.table_ref = bf16[32,2,640]{2,1,0:T(2,128)(2,1)S(1)} async-done(((bf16[32,2,640]{2,1,0:T(2,128)(2,1)}), bf16[32,2,640]{2,1,0:T(2,128)(2,1)S(1)}, u32[]{:S(2)}, u32[]{:S(2)}) %all-to-all-start.4) | async-done | bytes 81952 | tf_op jit(solution)/shard_map/all_to_all | solution.py:383
  161.8 1.5 shard_map.214
  (41 shorter events, 1.0 us)
Async XLA Ops:
  34.0 24.8 %copy-start.1 = (bf16[1,2048,128]{2,1,0:T(8,128)(2,1)S(1)}, bf16[1,2048,128]{2,1,0:T(8,128)(2,1)}, u32[]{:S(2)}) copy-start(bf16[1,2048,128]{2,1,0:T(8,128)(2,1)} %param.37) | copy-start | bytes 1572868
  34.0 24.8 %copy-start.2 = (bf16[1,2048,128]{2,1,0:T(8,128)(2,1)S(1)}, bf16[1,2048,128]{2,1,0:T(8,128)(2,1)}, u32[]{:S(2)}) copy-start(bf16[1,2048,128]{2,1,0:T(8,128)(2,1)} %param.38) | copy-start | bytes 1572868
  34.1 24.8 %copy-start.3 = (bf16[1,128,2048]{2,1,0:T(8,128)(2,1)S(1)}, bf16[1,128,2048]{2,1,0:T(8,128)(2,1)}, u32[]{:S(2)}) copy-start(bf16[1,128,2048]{2,1,0:T(8,128)(2,1)} %param.39) | copy-start | bytes 1572868
  61.6 3.8 %copy-start.17 = (bf16[24,256]{1,0:T(8,128)(2,1)S(1)}, bf16[24,256]{1,0:T(8,128)(2,1)}, u32[]{:S(2)}) copy-start(bf16[24,256]{1,0:T(8,128)(2,1)} %get-tuple-element.11) | copy-start | bytes 36868
  61.6 54.3 %all-to-all-start.3 = ((bf16[16,320,128]{2,1,0:T(8,128)(2,1)}), bf16[16,320,128]{2,1,0:T(8,128)(2,1)S(1)}, u32[]{:S(2)}, u32[]{:S(2)}) async-start(bf16[16,320,128]{2,1,0:T(8,128)(2,1)} %shard_map.212), calls=%async_computation.3 | async-start | bytes 2621440 | tf_op jit(solution)/shard_map/all_to_all | solution.py:383
  65.3 47.5 %copy-start = (bf16[256,2048]{1,0:T(8,128)(2,1)S(1)}, bf16[256,2048]{1,0:T(8,128)(2,1)}, u32[]{:S(2)}) copy-start(bf16[256,2048]{1,0:T(8,128)(2,1)} %weight_ref.1) | copy-start | bytes 3145732
  65.3 47.5 %copy-start.4 = (bf16[256,256]{1,0:T(8,128)(2,1)S(1)}, bf16[256,256]{1,0:T(8,128)(2,1)}, u32[]{:S(2)}) copy-start(bf16[256,256]{1,0:T(8,128)(2,1)} %gate_ref.1) | copy-start | bytes 393220
  65.4 47.5 %copy-start.9 = (f32[256,4]{0,1:T(4,128)S(1)}, f32[256,4]{0,1:T(4,128)}, u32[]{:S(2)}) copy-start(f32[256,4]{0,1:T(4,128)} %param.24) | copy-start | bytes 12292
  65.4 47.4 %copy-start.10 = (f32[256,4]{0,1:T(4,128)S(1)}, f32[256,4]{0,1:T(4,128)}, u32[]{:S(2)}) copy-start(f32[256,4]{0,1:T(4,128)} %param.25) | copy-start | bytes 12292
  65.4 47.4 %copy-start.12 = (f32[4]{0:T(128)S(1)}, f32[4]{0:T(128)}, u32[]{:S(2)}) copy-start(f32[4]{0:T(128)} %param.29) | copy-start | bytes 52
  65.4 47.4 %copy-start.13 = (f32[256]{0:T(256)S(1)}, f32[256]{0:T(256)}, u32[]{:S(2)}) copy-start(f32[256]{0:T(256)} %param.31) | copy-start | bytes 3076
  65.4 47.4 %copy-start.15 = (f32[4]{0:T(128)S(1)}, f32[4]{0:T(128)}, u32[]{:S(2)}) copy-start(f32[4]{0:T(128)} %param.30) | copy-start | bytes 52
  65.4 6.0 %collective-permute-start = (bf16[24,256]{1,0:T(8,128)(2,1)S(1)}, bf16[24,256]{1,0:T(8,128)(2,1)S(1)}, u32[]{:S(2)}, u32[]{:S(2)}) collective-permute-start(bf16[24,256]{1,0:T(8,128)(2,1)S(1)} %copy-done.17), channel_id=1, source_target_pairs={{0,16},{16,32},{32,48},{48,64},{64,80},{80,96},{96,112},{112,128},... | collective-permute-start | bytes 36872 | tf_op jit(solution)/shard_map/ppermute | solution.py:434
  71.5 0.6 copy-start.16
  75.8 37.0 %copy-start.5 = (bf16[256,256]{1,0:T(8,128)(2,1)S(1)}, bf16[256,256]{1,0:T(8,128)(2,1)}, u32[]{:S(2)}) copy-start(bf16[256,256]{1,0:T(8,128)(2,1)} %get-tuple-element.12.x_ref) | copy-start | bytes 393220
  75.8 37.0 %copy-start.6 = (bf16[256,256]{1,0:T(8,128)(2,1)S(1)}, bf16[256,256]{1,0:T(8,128)(2,1)}, u32[]{:S(2)}) copy-start(bf16[256,256]{1,0:T(8,128)(2,1)} %get-tuple-element.13.b_ref) | copy-start | bytes 393220
  75.9 37.0 %copy-start.7 = (bf16[256,256]{1,0:T(8,128)(2,1)S(1)}, bf16[256,256]{1,0:T(8,128)(2,1)}, u32[]{:S(2)}) copy-start(bf16[256,256]{1,0:T(8,128)(2,1)} %get-tuple-element.14.c_ref) | copy-start | bytes 393220
  75.9 37.0 %copy-start.8 = (f32[256,128]{1,0:T(8,128)S(1)}, f32[256,128]{1,0:T(8,128)}, u32[]{:S(2)}) copy-start(f32[256,128]{1,0:T(8,128)} %get-tuple-element.15.first_ref) | copy-start | bytes 393220
  78.3 5.0 %collective-permute-start.1 = (bf16[144,128]{1,0:T(8,128)(2,1)S(1)}, bf16[144,128]{1,0:T(8,128)(2,1)S(1)}, u32[]{:S(2)}, u32[]{:S(2)}) collective-permute-start(bf16[144,128]{1,0:T(8,128)(2,1)S(1)} %shard_map.205.own_ref), channel_id=1, source_target_pairs={{0,32},{32,64},{64,96},{96,128},{128,160},{160,192},{192,224},{224... | collective-permute-start | bytes 110600 | tf_op jit(solution)/shard_map/ppermute | solution.py:457
  83.5 5.4 %collective-permute-start.2 = (bf16[144,128]{1,0:T(8,128)(2,1)S(1)}, bf16[144,128]{1,0:T(8,128)(2,1)S(1)}, u32[]{:S(2)}, u32[]{:S(2)}) collective-permute-start(bf16[144,128]{1,0:T(8,128)(2,1)S(1)} %shard_map.206.own_ref), channel_id=1, source_target_pairs={{0,64},{32,96},{64,128},{96,160},{128,192},{160,224},{192,256},{22... | collective-permute-start | bytes 110600 | tf_op jit(solution)/shard_map/ppermute | solution.py:457
  115.9 23.3 %all-to-all-start = ((bf16[16,256,128]{2,1,0:T(8,128)(2,1)}), bf16[16,256,128]{2,1,0:T(8,128)(2,1)S(1)}, u32[]{:S(2)}, u32[]{:S(2)}) async-start(bf16[16,256,128]{2,1,0:T(8,128)(2,1)} %shard_map.209), calls=%async_computation | async-start | bytes 2097152 | tf_op jit(solution)/shard_map/all_to_all | solution.py:383
  122.8 39.0 %copy-start.11 = (s32[128,2]{0,1:T(2,128)S(1)}, s32[128,2]{0,1:T(2,128)}, u32[]{:S(2)}) copy-start(s32[128,2]{0,1:T(2,128)} %param.34) | copy-start | bytes 3076
  122.9 39.0 %copy-start.14 = (f32[128,2]{0,1:T(2,128)S(1)}, f32[128,2]{0,1:T(2,128)}, u32[]{:S(2)}) copy-start(f32[128,2]{0,1:T(2,128)} %param.35) | copy-start | bytes 3076
  139.2 22.6 %all-to-all-start.4 = ((bf16[32,2,640]{2,1,0:T(2,128)(2,1)}), bf16[32,2,640]{2,1,0:T(2,128)(2,1)S(1)}, u32[]{:S(2)}, u32[]{:S(2)}) async-start(bf16[32,2,640]{2,1,0:T(2,128)(2,1)} %shard_map.213), calls=%async_computation.4 | async-start | bytes 163840 | tf_op jit(solution)/shard_map/all_to_all | solution.py:383

commit v4 on v2

--- a/solution.py
+++ b/solution.py
@@ -9,8 +9,7 @@
 HEAD_DIM = 64
 STATE = 128
 BLOCK = 128
-CHIPS = "ep_0"
-EP = (CHIPS, "core")
+EP = ("ep_hi", "ep_lo", "core")
 LANES = 128
 PACK = 2
 NOTE = 16
@@ -60,7 +59,8 @@
     return whole
 
 
-def kernel_call(body, outs, args, flops, scratch=(), far=(), late=(), tails=(), vmem=VMEM):
+def kernel_call(body, outs, args, flops, scratch=(), far=(), late=(), tails=(), vmem=VMEM, out=None):
+    out = out or [pltpu.VMEM] * len(outs)
     size = sum(a.size * a.dtype.itemsize for a in args)
     size += sum(o.size * o.dtype.itemsize for o in outs)
     specs = [
@@ -77,7 +77,7 @@
         body,
         out_shape=outs,
         in_specs=specs,
-        out_specs=[pl.BlockSpec(memory_space=pltpu.VMEM)] * len(outs),
+        out_specs=[pl.BlockSpec(memory_space=kind) for kind in out],
         scratch_shapes=scratch,
         cost_estimate=pl.CostEstimate(flops=flops, bytes_accessed=size, transcendentals=0),
         compiler_params=pltpu.CompilerParams(vmem_limit_bytes=vmem),
@@ -113,16 +113,16 @@
 def pack_rows(rows, held, out_ref):
     experts = out_ref.shape[0]
     span = PACK * experts
-    for k in range(out_ref.shape[2] // LANES):
+    for k in range(rows.shape[0] // span):
         held[:, k * LANES : (k + 1) * LANES] = rows[k * span : (k + 1) * span, :]
     for e in range(experts):
         out_ref[e] = held[PACK * e : PACK * (e + 1), :]
 
 
-def unpack_rows(in_ref, held):
+def unpack_rows(in_ref, held, width):
     for e in range(in_ref.shape[0]):
         held[PACK * e : PACK * (e + 1), :] = in_ref[e]
-    parts = [held[:, k : k + LANES] for k in range(0, in_ref.shape[2], LANES)]
+    parts = [held[:, k : k + LANES] for k in range(0, width, LANES)]
     return jnp.concatenate(parts, axis=0)
 
 
@@ -132,7 +132,8 @@
 
 
 def dispatch_body(
-    tok_ref, gain_ref, routing_ref, x_ref, b_ref, c_ref, out_ref, edge_ref, held
+    tok_ref, gain_ref, routing_ref, x_ref, b_ref, c_ref, step_ref, extra_ref, rate_ref,
+    out_ref, edge_ref, held, wide_ref,
 ):
     tokens, model = tok_ref.shape
     rows = tok_ref[...].astype(F32)
@@ -140,21 +141,38 @@
     columns = pl.ds(pl.multiple_of(lax.axis_index("tp") * 128, 128), 128)
     own = (tok_ref[:, columns].astype(F32) * scale * gain_ref[:, columns]).astype(BF16)
     experts = out_ref.shape[0]
+    width = out_ref.shape[2] - LANES
+    _, log = log_decay_of(step_ref, extra_ref, rate_ref)
+    log = jnp.sum(log, axis=0, keepdims=True)
+    high = log.astype(BF16).astype(F32)
+    wide_ref[...] = jnp.zeros_like(wide_ref)
+    wide_ref[0:1, 0 : log.shape[1]] = high
+    wide_ref[1:2, 0 : log.shape[1]] = log - high
+    first = iota((experts * PACK, LANES), 0) % PACK == 0
+    held[:, width:] = jnp.where(first, wide_ref[0:1, :], wide_ref[1:2, :]).astype(BF16)
     slots = slots_of(routing_ref, experts)
-    place = iota((tokens, out_ref.shape[1] * experts * out_ref.shape[2] // LANES), 1)
+    place = iota((tokens, PACK * experts * width // LANES), 1)
     pick = jnp.where((place == slots[0]) | (place == slots[1]), 1.0, 0.0).astype(BF16)
     pack_rows(dot(pick, own, 0, 0).astype(BF16), held, out_ref)
     for k, ref in enumerate((x_ref, b_ref, c_ref)):
         edge_ref[8 * k : 8 * k + 8, :] = ref[...]
 
 
-def spread_body(in_ref, out_ref, held):
-    packed = unpack_rows(in_ref, held)
-    for peer in range(out_ref.shape[0]):
-        out_ref[peer] = packed
-
-
-def ffn_body(in_ref, gate_ref, up_ref, down_ref, out_ref, wait):
+def spread_body(in_ref, out_ref, log_ref, held, packed, sems):
+    width = in_ref.shape[2] - LANES
+    packed[...] = unpack_rows(in_ref, held, width)
+    log_ref[...] = held[:, width:]
+    copies = [
+        pltpu.make_async_copy(packed, out_ref.at[peer], sems.at[peer])
+        for peer in range(out_ref.shape[0])
+    ]
+    for copy in copies:
+        copy.start()
+    for copy in copies:
+        copy.wait()
+
+
+def ffn_body(in_ref, gate_ref, up_ref, down_ref, out_ref, held, sems, wait):
     parts, rows, width = in_ref.shape
     total = jnp.zeros((rows, 2 * width), F32)
     for k in range(0, parts, 2):
@@ -164,10 +182,18 @@
         total = total + dot(left, right)
     hidden = (silu(total[:, :width]) * total[:, width:]).astype(BF16)
     wait()
+    copies = []
     for k in range(0, parts, 2):
         value = dot(hidden, down_ref[:, k * width : (k + 2) * width]).astype(BF16)
-        out_ref[k] = value[:, :width]
-        out_ref[k + 1] = value[:, width:]
+        held[k] = value[:, :width]
+        held[k + 1] = value[:, width:]
+        if copies:
+            copies[-1].start()
+        both = pl.ds(k, 2)
+        copies.append(pltpu.make_async_copy(held.at[both], out_ref.at[both], sems.at[k // 2]))
+    copies[-1].start()
+    for copy in copies:
+        copy.wait()
 
 
 def sum_of(in_ref):
@@ -189,7 +215,7 @@
     tokens = routing_ref.shape[1]
     scores = upright(score_ref)
     whole = scores[:, 0:1] + scores[:, 1:2]
-    table = unpack_rows(table_ref, held)
+    table = unpack_rows(table_ref, held, table_ref.shape[2])
     place = iota((tokens, table.shape[0]), 1)
     total = jnp.zeros(out_ref.shape, F32)
     for index, slot in enumerate(slots_of(routing_ref, table_ref.shape[0])):
@@ -234,12 +260,11 @@
 
 
 def states_body(
-    x_ref, b_ref, c_ref, prior_ref, xt_ref, bt_ref, ct_ref, step_ref, extra_ref, rate_ref,
-    xo_ref, bo_ref, co_ref, first_ref, total_ref, held, wide_ref,
+    x_ref, b_ref, prior_ref, xt_ref, bt_ref, step_ref, extra_ref, rate_ref,
+    xo_ref, bo_ref, first_ref, total_ref, held, wide_ref,
 ):
     xo_ref[...] = conv_silu(x_ref, prior_ref, xt_ref, 0, held)
     bo_ref[...] = conv_silu(b_ref, prior_ref, bt_ref, 8, held)
-    co_ref[...] = conv_silu(c_ref, prior_ref, ct_ref, 16, held)
     step_all, log_all = log_decay_of(step_ref, extra_ref, rate_ref)
     wide = (BLOCK, 128)
     for group in range(x_ref.shape[1] // 128):
@@ -311,18 +336,40 @@
     write(out_ref, joined(read_half(both_ref, 0), read_half(both_ref, 1)), wide_ref)
 
 
-def join_first_body(came_ref, own_ref, out_ref, wide_ref):
-    write(out_ref, joined(read(came_ref[...]), read(own_ref[...])), wide_ref)
-
-
-def join_body(came_ref, own_ref, before_ref, out_ref, new_ref, wide_ref):
-    came = read(came_ref[...])
-    write(out_ref, joined(came, read(own_ref[...])), wide_ref)
-    write(new_ref, joined(came, read(before_ref[...])), wide_ref)
-
-
-def join_last_body(came_ref, before_ref, out_ref):
-    out_ref[...] = joined(read(came_ref[...]), read(before_ref[...]))[0]
+def join_far_body(far_ref, own_ref, log_ref, out_ref):
+    rows = far_ref.shape[1] - NOTE
+    group, place, core = (lax.axis_index(axis) for axis in EP)
+    device = iota(log_ref.shape, 0) // PACK
+    logs = log_ref[...].astype(F32)
+    heads = rows // HEAD_DIM
+
+    def decay(start, end):
+        log = jnp.where((device >= start) & (device < end), logs, 0.0)
+        log = jnp.sum(log, axis=0, keepdims=True)
+        log = jnp.where(core == 0, log[:, :heads], log[:, heads : 2 * heads])
+        return by_row(jnp.exp(log), rows)
+
+    groups, stride = far_ref.shape[0], log_ref.shape[0] // PACK // far_ref.shape[0]
+    upto = 2 * place + 2
+    state = jnp.zeros((rows, 128), F32)
+    for k in range(groups - 1):
+        new = state * decay(stride * (k - 1) + upto, stride * k + upto)
+        state = jnp.where(k < group, new + far_ref[k, :rows, :].astype(F32), state)
+    state = state * decay(stride * (group - 1) + upto, stride * group)
+    out_ref[0, :rows, :] = state.astype(BF16)
+    out_ref[0, rows:, :] = jnp.zeros((NOTE, 128), BF16)
+    out_ref[1] = own_ref[...]
+
+
+def join_near_body(near_ref, out_ref):
+    rows = near_ref.shape[2] - NOTE
+    place = lax.axis_index(EP[1])
+    state = near_ref[0, 0, :rows, :].astype(F32)
+    for k in range(1, near_ref.shape[0]):
+        state = state + near_ref[k, 0, :rows, :].astype(F32)
+    for k in range(near_ref.shape[0] - 1):
+        state = jnp.where(k < place, joined((state, 0.0), read(near_ref[k, 1]))[0], state)
+    out_ref[...] = state
 
 
 def income_of(chips_ref, both_ref):
@@ -332,9 +379,10 @@
 
 
 def mixer_body(
-    x_ref, b_ref, c_ref, gate_ref, first_ref, chips_ref, both_ref, step_ref, extra_ref,
-    rate_ref, skip_ref, gain_ref, weight_ref, out_ref, normed, income_ref,
+    x_ref, b_ref, projection_ref, prior_ref, taps_ref, gate_ref, first_ref, chips_ref, both_ref, step_ref, extra_ref,
+    rate_ref, skip_ref, gain_ref, weight_ref, out_ref, normed, income_ref, c_ref, held,
 ):
+    c_ref[...] = conv_silu(projection_ref, prior_ref, taps_ref, 16, held)
     income_ref[...] = income_of(chips_ref, both_ref)
     step_all, log_all = log_decay_of(step_ref, extra_ref, rate_ref)
     wide = (BLOCK, 128)
@@ -407,7 +455,9 @@
     top = routing.shape[1]
     capacity = (tokens * top * 5 + 4 * devices - 1) // (4 * devices)
     message = (devices, PACK, capacity // PACK * LANES)
+    noted = (*message[:2], message[2] + LANES)
     folded = pltpu.VMEM((devices * PACK, message[2]), BF16)
+    wider = pltpu.VMEM((devices * PACK, noted[2]), BF16)
     slots = devices * capacity
     rate, skip = decay_rate_log[None], head_skip_weight[None]
     step_rows, extra_rows = step_size_logits.T, extra_log_decay.T
@@ -415,14 +465,15 @@
 
     outgoing, edge = kernel_call(
         dispatch_body,
-        [shape(message, BF16), shape((24, channels), BF16)],
+        [shape(noted, BF16), shape((24, channels), BF16)],
         (
             expert_input_tokens, expert_norm_gain[None], routing_rows,
             mixer_input_channels, input_state_projection, output_state_projection,
+            step_rows, extra_rows, rate,
         ),
         2 * slots * tokens * 128,
-        [folded],
-        far=(0, 1, 2, 3, 4, 5),
+        [wider, pltpu.VMEM((8, LANES), F32)],
+        far=(0, 1, 2, 3, 4, 5, 6, 7, 8),
         tails=(3, 4, 5),
         vmem=WHOLE_VMEM,
     )
@@ -431,61 +482,54 @@
 
     note = channels + NOTE
     wide = pltpu.VMEM((NOTE, 128), F32)
-    x_conv, b_conv, c_conv, first, total = kernel_call(
+    x_conv, b_conv, first, total = kernel_call(
         states_body,
-        [shape((length, channels), BF16)] * 3
+        [shape((length, channels), BF16)] * 2
         + [shape((channels, STATE), F32), shape((note, STATE), BF16)],
         (
-            mixer_input_channels, input_state_projection, output_state_projection, prior,
-            mixer_channel_taps, input_state_taps, output_state_taps,
-            step_rows, extra_rows, rate,
+            mixer_input_channels, input_state_projection, prior,
+            mixer_channel_taps, input_state_taps, step_rows, extra_rows, rate,
         ),
         2 * length * channels * STATE,
         [pltpu.VMEM((length + 8, channels), F32), wide],
-        far=(0, 1, 2, 4, 5, 6, 7, 8, 9),
+        far=(0, 1, 3, 4, 5, 6, 7),
         vmem=WHOLE_VMEM,
     )
 
-    def moved(value, distance):
-        chips = lax.axis_size(CHIPS)
-        route = [(i, i + distance) for i in range(chips - distance)]
-        return lax.ppermute(value, CHIPS, route)
-
-    half = channels // 2
-    carried = shape((half + NOTE, STATE), BF16)
-
-    def join(body, values, more=()):
-        outs = [carried, *more]
-        return kernel_call(body, outs, values, 4 * channels * STATE, [wide])
-
-    both = lax.all_gather(total, "core")
-    (upto,) = join(join_core_body, (both,))
-    before = came = moved(upto, 1)
-    (upto,) = join(join_first_body, (came, upto))
-    for distance in (2, 4):
-        came = moved(upto, distance)
-        upto, before = join(join_body, (came, upto, before), [shape(carried.shape, F32)])
-    (chips,) = kernel_call(
-        join_last_body, [shape((half, STATE), F32)], (moved(upto, 8), before), 4 * half * STATE
-    )
-    chips = lax.all_gather(chips, "core", tiled=True)
-
-    (copies,) = kernel_call(
+    (copies, logs) = kernel_call(
         spread_body,
-        [shape((parts, devices * capacity, 128), BF16)],
+        [shape((parts, slots, 128), BF16), shape((devices * PACK, LANES), BF16)],
         (arrived,),
         parts * slots * 128,
-        [folded],
+        [wider, pltpu.VMEM((slots, 128), BF16), pltpu.SemaphoreType.DMA((parts,))],
+        out=(pltpu.HBM, pltpu.VMEM),
     )
     gathered = all_to_all(copies, "tp")
+
+    half = channels // 2
+    carried = (half + NOTE, STATE)
+    both = lax.all_gather(total, "core")
+    (chip,) = kernel_call(join_core_body, [shape(carried, BF16)], (both,), 4 * half * STATE, [wide])
+    far = lax.all_gather(chip, EP[0])
+    (earlier,) = kernel_call(
+        join_far_body, [shape((2, *carried), BF16)], (far, chip, logs), 8 * half * STATE
+    )
+    near = lax.all_gather(earlier, EP[1])
+    (chips,) = kernel_call(join_near_body, [shape((half, STATE), F32)], (near,), 8 * half * STATE)
+    chips = lax.all_gather(chips, "core", tiled=True)
 
     (partial_rows,) = kernel_call(
         ffn_body,
         [shape((parts, devices * capacity, 128), BF16)],
         (gathered, expert_gate_weight[0], expert_up_weight[0], expert_down_weight[0]),
         6 * devices * capacity * model * 128,
+        [
+            pltpu.VMEM((parts, slots, 128), BF16),
+            pltpu.SemaphoreType.DMA((parts // 2,)),
+        ],
         far=(3,),
         late=(3,),
+        out=(pltpu.HBM,),
     )
     expert_parts = all_to_all(partial_rows, "tp")
 
@@ -493,11 +537,14 @@
         mixer_body,
         [shape((parts, length, 128), BF16)],
         (
-            x_conv, b_conv, c_conv, output_gate_logits, first, chips, both,
+            x_conv, b_conv, output_state_projection, prior, output_state_taps, output_gate_logits, first, chips, both,
             step_rows, extra_rows, rate, skip, grouped_norm_gain[None], mixer_output_weight,
         ),
         2 * length * channels * model,
-        [pltpu.VMEM((length, channels), BF16), pltpu.VMEM((channels, STATE), F32)],
+        [
+            pltpu.VMEM((length, channels), BF16), pltpu.VMEM((channels, STATE), F32),
+            pltpu.VMEM((length, channels), BF16), pltpu.VMEM((length + 8, channels), F32),
+        ],
     )
     mixer_parts = all_to_all(mixer_part, "tp")
 
@@ -520,7 +567,7 @@
 
 
 def solution(mesh):
-    split = Mesh(mesh.devices.reshape(16, 2, mesh.shape["tp"]), (*EP, "tp"))
+    split = Mesh(mesh.devices.reshape(4, 4, 2, mesh.shape["tp"]), (*EP, "tp"))
     in_specs = (
         P(EP, "tp"),
         P(EP, "tp"),

time: 174 us -> 166 us (0.954)
  starting transfers between devices: 55.7 us -> 23.8 us
  blocking collectives: 62.7 us -> 93.7 us
  waiting for transfers between devices: 33.4 us -> 29.2 us
  local copies, waits for them, and re-layouts: 4.29 us -> 0.71 us
    all_gather x0 -> x2, blocking collectives: none -> 27.1 us  [the longest x1 14.8 us: per_device(): far = lax.all_gather(chip, EP[0])]
    ppermute x4 -> x0, starting transfers between devices: 25.1 us -> none  [moved(): return lax.ppermute(value, CHIPS, route)]
    all_to_all x3, starting transfers between devices: 25.3 us -> 19.4 us  [all_to_all(): return lax.all_to_all(value, axis, split_axis=0, concat_axis=0, tiled=True)]
    ppermute x4 -> x0, waiting for transfers between devices: 4.17 us -> none  [moved(): return lax.ppermute(value, CHIPS, route)]
    unnamed x36 -> x40, local copies, waits for them, and re-layouts: 4.29 us -> 0.71 us
    all_gather x1, blocking collectives: 5.37 us -> 7.83 us  [per_device(): chips = lax.all_gather(chips, 'core', tiled=True)]
    pallas_call x13 -> x11, Pallas kernels: 16.3 us -> 17.3 us  [kernel_call(): pl.pallas_call(body, out_shape=outs, in_specs=specs, out_specs=[pl.BlockS...]
  transfers between devices with their start and end apart: 8 -> 4, of which waited for: 7 -> 3; matrix products, arithmetic and copies ran while one was open for 0% -> 0% of each run, Pallas kernels for 5% -> 5%
where the time goes in v4:
time: 166 us
  blocking collectives  93.7 us (56%)
  waiting for transfers between devices  29.2 us (18%)
  starting transfers between devices  23.8 us (14%)
  Pallas kernels  17.3 us (10%)
    all_to_all x2, blocking collectives, all_to_all(): return lax.all_to_all(value, axis, split_axis=0, concat_axis=0, tiled=True)  56.6 us
    all_to_all x3, waiting for transfers between devices, all_to_all(): return lax.all_to_all(value, axis, split_axis=0, concat_axis=0, tiled=True)  28.4 us
    all_to_all x3, starting transfers between devices, all_to_all(): return lax.all_to_all(value, axis, split_axis=0, concat_axis=0, tiled=True)  19.4 us
    pallas_call x11, Pallas kernels, kernel_call(): pl.pallas_call(body, out_shape=outs, in_specs=specs, out_specs=[pl.BlockS...  17.3 us
    all_gather x1, blocking collectives, per_device(): far = lax.all_gather(chip, EP[0])  14.8 us
    all_gather x1, blocking collectives, per_device(): near = lax.all_gather(earlier, EP[1])  12.3 us
    all_gather x1, blocking collectives, per_device(): chips = lax.all_gather(chips, 'core', tiled=True)  7.83 us
    ppermute x1, starting transfers between devices, per_device(): prior = lax.ppermute(edge, EP, [(i, i + 1) for i in range(devices - 1)])  4.4 us
  transfers between devices with their start and end apart: 4, of which 3 were waited for; matrix products, arithmetic and copies ran while one was open for 0% of the time, Pallas kernels for 5%

profile of v4, /device:TPU:1, one launch (start us, length us, event | category | flops | bytes accessed | tf_op | source)
XLA Modules:
  0.0 165.6 jit_solution(6772710004653176505)
XLA Ops:
  0.6 2.7 %shard_map.203 = (bf16[32,2,768]{2,1,0:T(2,128)(2,1)}, bf16[24,256]{1,0:T(8,128)(2,1)}) custom-call(bf16[128,2048]{1,0:T(8,128)(2,1)} %refs_0_.2, f32[1,2048]{1,0:T(1,128)} %bitcast.35, s32[2,128]{1,0:T(2,128)} %bitcast.30, bf16[256,256]{1,0:T(8,128)(2,1)} %refs_0_.3, bf16[256,256]{1,0:T(8,128)(2,1)} %refs_1_.1, bf16[256,256]{1,0:T(8,128)(2,1)} %projection_ref.1, ...), custom_call_target="tpu_custom_call" | custom-call | flops 10485760 | bytes 1045520 | tf_op jit(solution)/shard_map/pallas_call | solution.py:76
  3.3 31.5 %all_to_all.25.in_ref = bf16[32,2,768]{2,1,0:T(2,128)(2,1)S(1)} all-to-all(bf16[32,2,768]{2,1,0:T(2,128)(2,1)} %get-tuple-element.15), channel_id=1, replica_groups=mesh['ep_hi'=4,'ep_lo'=4,'core'=2,'tp'=16] {'ep_hi','ep_lo','core'}, dimensions={0} | all-to-all | bytes 196608 | tf_op jit(solution)/shard_map/all_to_all | solution.py:426
  34.8 1.9 %shard_map.206 = (bf16[16,320,128]{2,1,0:T(8,128)(2,1)S(1)}, bf16[64,128]{1,0:T(8,128)(2,1)S(1)}) custom-call(bf16[32,2,768]{2,1,0:T(2,128)(2,1)S(1)} %all_to_all.25.in_ref), custom_call_target="tpu_custom_call" | custom-call | flops 655360 | bytes 1425408 | tf_op jit(solution)/shard_map/pallas_call | solution.py:76
  36.7 25.1 %all_to_all.26.refs_0_ = bf16[16,320,128]{2,1,0:T(8,128)(2,1)S(1)} all-to-all(bf16[16,320,128]{2,1,0:T(8,128)(2,1)S(1)} %get-tuple-element.17), channel_id=1, replica_groups=mesh['ep_hi'=4,'ep_lo'=4,'core'=2,'tp'=16] {'tp'}, dimensions={0} | all-to-all | bytes 2621440 | tf_op jit(solution)/shard_map/all_to_all | solution.py:426
  61.8 2.5 %shard_map.211 = bf16[16,320,128]{2,1,0:T(8,128)(2,1)} custom-call(bf16[16,320,128]{2,1,0:T(8,128)(2,1)S(1)} %all_to_all.26.refs_0_, bf16[2048,128]{1,0:T(8,128)(2,1)S(1)} %bitcast.18, bf16[2048,128]{1,0:T(8,128)(2,1)S(1)} %bitcast.19, bf16[128,2048]{1,0:T(8,128)(2,1)S(1)} %bitcast.20), custom_call_target="tpu_custom_call" | custom-call | flops 503316480 | bytes 4194304 | tf_op jit(solution)/shard_map/pallas_call | solution.py:76
  64.4 3.7 %all-to-all-start.3 = ((bf16[16,320,128]{2,1,0:T(8,128)(2,1)}), bf16[16,320,128]{2,1,0:T(8,128)(2,1)S(1)}, u32[]{:S(2)}, u32[]{:S(2)}) async-start(bf16[16,320,128]{2,1,0:T(8,128)(2,1)} %shard_map.211), calls=%async_computation.3 | async-start | bytes 2621440 | tf_op jit(solution)/shard_map/all_to_all | solution.py:426
  68.2 4.4 %collective-permute-start = (bf16[24,256]{1,0:T(8,128)(2,1)S(1)}, bf16[24,256]{1,0:T(8,128)(2,1)S(1)}, u32[]{:S(2)}, u32[]{:S(2)}) collective-permute-start(bf16[24,256]{1,0:T(8,128)(2,1)S(1)} %copy-done.19), channel_id=1, source_target_pairs={{0,16},{16,32},{32,48},{48,64},{64,80},{80,96},{96,112},{112,128},... | collective-permute-start | bytes 36872 | tf_op jit(solution)/shard_map/ppermute | solution.py:480
  72.6 0.8 collective-permute-done.refs_2_.prior_ref
  73.4 0.6 copy-done.9
  74.0 3.4 %shard_map.204 = (bf16[256,256]{1,0:T(8,128)(2,1)}, bf16[256,256]{1,0:T(8,128)(2,1)}, f32[256,128]{1,0:T(8,128)}, bf16[272,128]{1,0:T(8,128)(2,1)}) custom-call(bf16[256,256]{1,0:T(8,128)(2,1)} %refs_0_.3, bf16[256,256]{1,0:T(8,128)(2,1)} %refs_1_.1, bf16[24,256]{1,0:T(8,128)(2,1)} %copy-done.9, bf16[4,256]{1,0:T(4,128)(2,1)} %refs_3_.3, ...), custom_call_target="tpu_custom_call" | custom-call | flops 16777216 | bytes 749584 | tf_op jit(solution)/shard_map/pallas_call | solution.py:76
  77.5 2.2 %all-gather = bf16[544,128]{1,0:T(8,128)(2,1)S(1)} all-gather(bf16[272,128]{1,0:T(8,128)(2,1)} %get-tuple-element.14), channel_id=2, replica_groups=mesh['ep_hi'=4,'ep_lo'=4,'core'=2,'tp'=16] {'core'}, dimensions={0}, use_global_device_ids=true | all-gather | bytes 208896 | tf_op jit(solution)/shard_map/all_gather | solution.py:511
  79.8 0.2 shard_map.205.own_ref
  79.9 14.8 %all-gather.1 = bf16[576,128]{1,0:T(8,128)(2,1)S(1)} all-gather(bf16[144,128]{1,0:T(8,128)(2,1)S(1)} %shard_map.205.own_ref), channel_id=3, replica_groups=mesh['ep_hi'=4,'ep_lo'=4,'core'=2,'tp'=16] {'ep_hi'}, dimensions={0}, use_global_device_ids=true | all-gather | bytes 184320 | tf_op jit(solution)/shard_map/all_gather | solution.py:513
  94.7 0.2 shard_map.207
  95.0 12.3 %all-gather.2 = bf16[8,144,128]{2,1,0:T(8,128)(2,1)S(1)} all-gather(bf16[2,144,128]{2,1,0:T(8,128)(2,1)S(1)} %shard_map.207), channel_id=4, replica_groups=mesh['ep_hi'=4,'ep_lo'=4,'core'=2,'tp'=16] {'ep_lo'}, dimensions={0}, use_global_device_ids=true | all-gather | bytes 368640 | tf_op jit(solution)/shard_map/all_gather | solution.py:517
  107.4 7.8 %all_gather.27.chips_ref = f32[256,128]{1,0:T(8,128)S(1)} all-gather(f32[128,128]{1,0:T(8,128)S(1)} %shard_map.208), channel_id=1, replica_groups=mesh['ep_hi'=4,'ep_lo'=4,'core'=2,'tp'=16] {'core'}, dimensions={0}, use_global_device_ids=true | all-gather | bytes 196608 | tf_op jit(solution)/shard_map/all_gather | solution.py:519
  115.3 3.1 %shard_map.209 = bf16[16,256,128]{2,1,0:T(8,128)(2,1)} custom-call(bf16[256,256]{1,0:T(8,128)(2,1)S(1)} %copy-done.6, bf16[256,256]{1,0:T(8,128)(2,1)S(1)} %copy-done.7, bf16[256,256]{1,0:T(8,128)(2,1)S(1)} %copy-done.1, bf16[24,256]{1,0:T(8,128)(2,1)S(1)} %copy-done.10, bf16[4,256]{1,0:T(4,128)(2,1)S(1)} %copy-done.15, bf16[256,256]{1,0:T(8,128)(2,1)S(1)} %copy-done.5, ...), custom_call_target="tpu_custom_call" | custom-call | flops 268435456 | bytes 3046432 | tf_op jit(solution)/shard_map/pallas_call | solution.py:76
  118.4 6.8 %all-to-all-start.1 = ((bf16[16,256,128]{2,1,0:T(8,128)(2,1)}), bf16[16,256,128]{2,1,0:T(8,128)(2,1)S(1)}, u32[]{:S(2)}, u32[]{:S(2)}) async-start(bf16[16,256,128]{2,1,0:T(8,128)(2,1)} %shard_map.209), calls=%async_computation.1 | async-start | bytes 2097152 | tf_op jit(solution)/shard_map/all_to_all | solution.py:426
  125.2 0.9 shard_map.212
  126.1 15.4 %all-to-all-done.1.in_ref = bf16[16,256,128]{2,1,0:T(8,128)(2,1)S(1)} async-done(((bf16[16,256,128]{2,1,0:T(8,128)(2,1)}), bf16[16,256,128]{2,1,0:T(8,128)(2,1)S(1)}, u32[]{:S(2)}, u32[]{:S(2)}) %all-to-all-start.1) | async-done | bytes 1048608 | tf_op jit(solution)/shard_map/all_to_all | solution.py:426
  141.6 8.9 %all-to-all-start.4 = ((bf16[32,2,640]{2,1,0:T(2,128)(2,1)}), bf16[32,2,640]{2,1,0:T(2,128)(2,1)S(1)}, u32[]{:S(2)}, u32[]{:S(2)}) async-start(bf16[32,2,640]{2,1,0:T(2,128)(2,1)} %shard_map.212), calls=%async_computation.4 | async-start | bytes 163840 | tf_op jit(solution)/shard_map/all_to_all | solution.py:426
  150.5 0.8 shard_map.210
  151.2 12.9 %all-to-all-done.4.table_ref = bf16[32,2,640]{2,1,0:T(2,128)(2,1)S(1)} async-done(((bf16[32,2,640]{2,1,0:T(2,128)(2,1)}), bf16[32,2,640]{2,1,0:T(2,128)(2,1)S(1)}, u32[]{:S(2)}, u32[]{:S(2)}) %all-to-all-start.4) | async-done | bytes 81952 | tf_op jit(solution)/shard_map/all_to_all | solution.py:426
  164.2 1.5 shard_map.213
  (41 shorter events, 0.3 us)
Async XLA Ops:
  36.7 25.1 %copy-start.2 = (bf16[1,2048,128]{2,1,0:T(8,128)(2,1)S(1)}, bf16[1,2048,128]{2,1,0:T(8,128)(2,1)}, u32[]{:S(2)}) copy-start(bf16[1,2048,128]{2,1,0:T(8,128)(2,1)} %param.37) | copy-start | bytes 1572868
  36.7 25.1 %copy-start.3 = (bf16[1,2048,128]{2,1,0:T(8,128)(2,1)S(1)}, bf16[1,2048,128]{2,1,0:T(8,128)(2,1)}, u32[]{:S(2)}) copy-start(bf16[1,2048,128]{2,1,0:T(8,128)(2,1)} %param.38) | copy-start | bytes 1572868
  36.7 25.1 %copy-start.4 = (bf16[1,128,2048]{2,1,0:T(8,128)(2,1)S(1)}, bf16[1,128,2048]{2,1,0:T(8,128)(2,1)}, u32[]{:S(2)}) copy-start(bf16[1,128,2048]{2,1,0:T(8,128)(2,1)} %param.39) | copy-start | bytes 1572868
  64.3 3.8 %copy-start.19 = (bf16[24,256]{1,0:T(8,128)(2,1)S(1)}, bf16[24,256]{1,0:T(8,128)(2,1)}, u32[]{:S(2)}) copy-start(bf16[24,256]{1,0:T(8,128)(2,1)} %get-tuple-element.10) | copy-start | bytes 36868
  64.4 54.1 %all-to-all-start.3 = ((bf16[16,320,128]{2,1,0:T(8,128)(2,1)}), bf16[16,320,128]{2,1,0:T(8,128)(2,1)S(1)}, u32[]{:S(2)}, u32[]{:S(2)}) async-start(bf16[16,320,128]{2,1,0:T(8,128)(2,1)} %shard_map.211), calls=%async_computation.3 | async-start | bytes 2621440 | tf_op jit(solution)/shard_map/all_to_all | solution.py:426
  68.1 47.1 %copy-start = (bf16[256,2048]{1,0:T(8,128)(2,1)S(1)}, bf16[256,2048]{1,0:T(8,128)(2,1)}, u32[]{:S(2)}) copy-start(bf16[256,2048]{1,0:T(8,128)(2,1)} %weight_ref.1) | copy-start | bytes 3145732
  68.1 47.1 %copy-start.1 = (bf16[256,256]{1,0:T(8,128)(2,1)S(1)}, bf16[256,256]{1,0:T(8,128)(2,1)}, u32[]{:S(2)}) copy-start(bf16[256,256]{1,0:T(8,128)(2,1)} %projection_ref.1) | copy-start | bytes 393220
  68.1 47.1 %copy-start.5 = (bf16[256,256]{1,0:T(8,128)(2,1)S(1)}, bf16[256,256]{1,0:T(8,128)(2,1)}, u32[]{:S(2)}) copy-start(bf16[256,256]{1,0:T(8,128)(2,1)} %gate_ref.1) | copy-start | bytes 393220
  68.1 47.1 %copy-start.11 = (f32[256,4]{0,1:T(4,128)S(1)}, f32[256,4]{0,1:T(4,128)}, u32[]{:S(2)}) copy-start(f32[256,4]{0,1:T(4,128)} %param.24) | copy-start | bytes 12292
  68.1 47.1 %copy-start.12 = (f32[256,4]{0,1:T(4,128)S(1)}, f32[256,4]{0,1:T(4,128)}, u32[]{:S(2)}) copy-start(f32[256,4]{0,1:T(4,128)} %param.25) | copy-start | bytes 12292
  68.1 47.1 %copy-start.13 = (f32[4]{0:T(128)S(1)}, f32[4]{0:T(128)}, u32[]{:S(2)}) copy-start(f32[4]{0:T(128)} %param.29) | copy-start | bytes 52
  68.1 47.1 %copy-start.15 = (bf16[4,256]{1,0:T(4,128)(2,1)S(1)}, bf16[4,256]{1,0:T(4,128)(2,1)}, u32[]{:S(2)}) copy-start(bf16[4,256]{1,0:T(4,128)(2,1)} %taps_ref.1) | copy-start | bytes 6148
  68.2 47.1 %copy-start.16 = (f32[256]{0:T(256)S(1)}, f32[256]{0:T(256)}, u32[]{:S(2)}) copy-start(f32[256]{0:T(256)} %param.31) | copy-start | bytes 3076
  68.2 47.1 %copy-start.18 = (f32[4]{0:T(128)S(1)}, f32[4]{0:T(128)}, u32[]{:S(2)}) copy-start(f32[4]{0:T(128)} %param.30) | copy-start | bytes 52
  68.2 5.2 %collective-permute-start = (bf16[24,256]{1,0:T(8,128)(2,1)S(1)}, bf16[24,256]{1,0:T(8,128)(2,1)S(1)}, u32[]{:S(2)}, u32[]{:S(2)}) collective-permute-start(bf16[24,256]{1,0:T(8,128)(2,1)S(1)} %copy-done.19), channel_id=1, source_target_pairs={{0,16},{16,32},{32,48},{48,64},{64,80},{80,96},{96,112},{112,128},... | collective-permute-start | bytes 36872 | tf_op jit(solution)/shard_map/ppermute | solution.py:480
  73.4 0.6 copy-start.9
  77.5 37.8 %copy-start.6 = (bf16[256,256]{1,0:T(8,128)(2,1)S(1)}, bf16[256,256]{1,0:T(8,128)(2,1)}, u32[]{:S(2)}) copy-start(bf16[256,256]{1,0:T(8,128)(2,1)} %get-tuple-element.11.x_ref) | copy-start | bytes 393220
  77.5 37.8 %copy-start.7 = (bf16[256,256]{1,0:T(8,128)(2,1)S(1)}, bf16[256,256]{1,0:T(8,128)(2,1)}, u32[]{:S(2)}) copy-start(bf16[256,256]{1,0:T(8,128)(2,1)} %get-tuple-element.12.b_ref) | copy-start | bytes 393220
  77.5 37.8 %copy-start.8 = (f32[256,128]{1,0:T(8,128)S(1)}, f32[256,128]{1,0:T(8,128)}, u32[]{:S(2)}) copy-start(f32[256,128]{1,0:T(8,128)} %get-tuple-element.13.first_ref) | copy-start | bytes 393220
  77.5 37.8 %copy-start.10 = (bf16[24,256]{1,0:T(8,128)(2,1)S(1)}, bf16[24,256]{1,0:T(8,128)(2,1)}, u32[]{:S(2)}) copy-start(bf16[24,256]{1,0:T(8,128)(2,1)} %copy-done.9) | copy-start | bytes 36868
  118.4 23.1 %all-to-all-start.1 = ((bf16[16,256,128]{2,1,0:T(8,128)(2,1)}), bf16[16,256,128]{2,1,0:T(8,128)(2,1)S(1)}, u32[]{:S(2)}, u32[]{:S(2)}) async-start(bf16[16,256,128]{2,1,0:T(8,128)(2,1)} %shard_map.209), calls=%async_computation.1 | async-start | bytes 2097152 | tf_op jit(solution)/shard_map/all_to_all | solution.py:426
  125.2 39.0 %copy-start.14 = (s32[128,2]{0,1:T(2,128)S(1)}, s32[128,2]{0,1:T(2,128)}, u32[]{:S(2)}) copy-start(s32[128,2]{0,1:T(2,128)} %param.34) | copy-start | bytes 3076
  125.2 39.0 %copy-start.17 = (f32[128,2]{0,1:T(2,128)S(1)}, f32[128,2]{0,1:T(2,128)}, u32[]{:S(2)}) copy-start(f32[128,2]{0,1:T(2,128)} %param.35) | copy-start | bytes 3076
  141.6 22.6 %all-to-all-start.4 = ((bf16[32,2,640]{2,1,0:T(2,128)(2,1)}), bf16[32,2,640]{2,1,0:T(2,128)(2,1)S(1)}, u32[]{:S(2)}, u32[]{:S(2)}) async-start(bf16[32,2,640]{2,1,0:T(2,128)(2,1)} %shard_map.212), calls=%async_computation.4 | async-start | bytes 163840 | tf_op jit(solution)/shard_map/all_to_all | solution.py:426

commit v5 on v4

--- a/solution.py
+++ b/solution.py
@@ -110,6 +110,21 @@
     return slots
 
 
+def slots_along(routing_ref, experts):
+    tokens = routing_ref.shape[1]
+    expert = iota((experts, tokens), 0)
+    named = [routing_ref[k : k + 1, :] for k in range(routing_ref.shape[0])]
+    chosen = [expert == name for name in named]
+    member = jnp.where(chosen[0] | chosen[1], 1.0, 0.0).astype(BF16)
+    earlier = jnp.where(iota((tokens, tokens), 0) < iota((tokens, tokens), 1), 1.0, 0.0)
+    place = dot(member, earlier.astype(BF16))
+    slots = []
+    for name, mask in zip(named, chosen):
+        rank = jnp.sum(jnp.where(mask, place, 0.0), axis=0, keepdims=True).astype(jnp.int32)
+        slots.append(rank // PACK * (PACK * experts) + name * PACK + rank % PACK)
+    return slots
+
+
 def pack_rows(rows, held, out_ref):
     experts = out_ref.shape[0]
     span = PACK * experts
@@ -133,15 +148,13 @@
 
 def dispatch_body(
     tok_ref, gain_ref, routing_ref, x_ref, b_ref, c_ref, step_ref, extra_ref, rate_ref,
-    out_ref, edge_ref, held, wide_ref,
+    out_ref, edge_ref, held, wide_ref, wait,
 ):
     tokens, model = tok_ref.shape
-    rows = tok_ref[...].astype(F32)
-    scale = lax.rsqrt(jnp.sum(rows * rows, axis=1, keepdims=True) * (1.0 / model) + eps)
-    columns = pl.ds(pl.multiple_of(lax.axis_index("tp") * 128, 128), 128)
-    own = (tok_ref[:, columns].astype(F32) * scale * gain_ref[:, columns]).astype(BF16)
     experts = out_ref.shape[0]
     width = out_ref.shape[2] - LANES
+    for k, ref in enumerate((x_ref, b_ref, c_ref)):
+        edge_ref[8 * k : 8 * k + 8, :] = ref[...]
     _, log = log_decay_of(step_ref, extra_ref, rate_ref)
     log = jnp.sum(log, axis=0, keepdims=True)
     high = log.astype(BF16).astype(F32)
@@ -150,12 +163,15 @@
     wide_ref[1:2, 0 : log.shape[1]] = log - high
     first = iota((experts * PACK, LANES), 0) % PACK == 0
     held[:, width:] = jnp.where(first, wide_ref[0:1, :], wide_ref[1:2, :]).astype(BF16)
-    slots = slots_of(routing_ref, experts)
-    place = iota((tokens, PACK * experts * width // LANES), 1)
+    slots = slots_along(routing_ref, experts)
+    place = iota((PACK * experts * width // LANES, tokens), 0)
     pick = jnp.where((place == slots[0]) | (place == slots[1]), 1.0, 0.0).astype(BF16)
-    pack_rows(dot(pick, own, 0, 0).astype(BF16), held, out_ref)
-    for k, ref in enumerate((x_ref, b_ref, c_ref)):
-        edge_ref[8 * k : 8 * k + 8, :] = ref[...]
+    wait()
+    rows = tok_ref[...].astype(F32)
+    scale = lax.rsqrt(jnp.sum(rows * rows, axis=1, keepdims=True) * (1.0 / model) + eps)
+    columns = pl.ds(pl.multiple_of(lax.axis_index("tp") * 128, 128), 128)
+    own = (tok_ref[:, columns].astype(F32) * scale * gain_ref[:, columns]).astype(BF16)
+    pack_rows(dot(pick, own).astype(BF16), held, out_ref)
 
 
 def spread_body(in_ref, out_ref, log_ref, held, packed, sems):
@@ -332,12 +348,14 @@
     return state, jnp.where(core == 0, log[:, :heads], log[:, heads:])
 
 
-def join_core_body(both_ref, out_ref, wide_ref):
-    write(out_ref, joined(read_half(both_ref, 0), read_half(both_ref, 1)), wide_ref)
+def join_core_body(both_ref, out_ref, state_ref, wide_ref):
+    chip = joined(read_half(both_ref, 0), read_half(both_ref, 1))
+    write(out_ref, chip, wide_ref)
+    state_ref[...] = chip[0].astype(BF16)
 
 
 def join_far_body(far_ref, own_ref, log_ref, out_ref):
-    rows = far_ref.shape[1] - NOTE
+    rows = far_ref.shape[1]
     group, place, core = (lax.axis_index(axis) for axis in EP)
     device = iota(log_ref.shape, 0) // PACK
     logs = log_ref[...].astype(F32)
@@ -474,6 +492,7 @@
         2 * slots * tokens * 128,
         [wider, pltpu.VMEM((8, LANES), F32)],
         far=(0, 1, 2, 3, 4, 5, 6, 7, 8),
+        late=(0,),
         tails=(3, 4, 5),
         vmem=WHOLE_VMEM,
     )
@@ -509,8 +528,9 @@
     half = channels // 2
     carried = (half + NOTE, STATE)
     both = lax.all_gather(total, "core")
-    (chip,) = kernel_call(join_core_body, [shape(carried, BF16)], (both,), 4 * half * STATE, [wide])
-    far = lax.all_gather(chip, EP[0])
+    outs = [shape(carried, BF16), shape((half, STATE), BF16)]
+    chip, state = kernel_call(join_core_body, outs, (both,), 4 * half * STATE, [wide])
+    far = lax.all_gather(state, EP[0])
     (earlier,) = kernel_call(
         join_far_body, [shape((2, *carried), BF16)], (far, chip, logs), 8 * half * STATE
     )

time: 166 us -> 166 us (level)
  no operation moved by 1% of the time
where the time goes in v5:
time: 166 us; the launch traced here: 165 us
  blocking collectives  93.6 us (56%)
  waiting for transfers between devices  29.2 us (18%)
  starting transfers between devices  23.5 us (14%)
  Pallas kernels  17 us (10%)
    all_to_all x2, blocking collectives, all_to_all(): return lax.all_to_all(value, axis, split_axis=0, concat_axis=0, tiled=True)  56.6 us
    all_to_all x3, waiting for transfers between devices, all_to_all(): return lax.all_to_all(value, axis, split_axis=0, concat_axis=0, tiled=True)  28.4 us
    all_to_all x3, starting transfers between devices, all_to_all(): return lax.all_to_all(value, axis, split_axis=0, concat_axis=0, tiled=True)  19.1 us
    pallas_call x11, Pallas kernels, kernel_call(): pl.pallas_call(body, out_shape=outs, in_specs=specs, out_specs=[pl.BlockS...  17 us
    all_gather x1, blocking collectives, per_device(): far = lax.all_gather(state, EP[0])  14.7 us
    all_gather x1, blocking collectives, per_device(): near = lax.all_gather(earlier, EP[1])  12.1 us
    all_gather x1, blocking collectives, per_device(): chips = lax.all_gather(chips, 'core', tiled=True)  7.91 us
    ppermute x1, starting transfers between devices, per_device(): prior = lax.ppermute(edge, EP, [(i, i + 1) for i in range(devices - 1)])  4.4 us
  transfers between devices with their start and end apart: 4, of which 3 were waited for; matrix products, arithmetic and copies ran while one was open for 0% of the time, Pallas kernels for 5%

profile of v5, /device:TPU:1, one launch (start us, length us, event | category | flops | bytes accessed | tf_op | source)
XLA Modules:
  0.0 165.0 jit_solution(6452064615177297615)
XLA Ops:
  0.6 2.3 %shard_map.203 = (bf16[32,2,768]{2,1,0:T(2,128)(2,1)}, bf16[24,256]{1,0:T(8,128)(2,1)}) custom-call(bf16[128,2048]{1,0:T(8,128)(2,1)} %refs_0_.2, f32[1,2048]{1,0:T(1,128)} %bitcast.35, s32[2,128]{1,0:T(2,128)} %bitcast.30, bf16[256,256]{1,0:T(8,128)(2,1)} %refs_0_.3, bf16[256,256]{1,0:T(8,128)(2,1)} %refs_1_.1, bf16[256,256]{1,0:T(8,128)(2,1)} %projection_ref.1, ...), custom_call_target="tpu_custom_call" | custom-call | flops 10485760 | bytes 1045520 | tf_op jit(solution)/shard_map/pallas_call | solution.py:76
  2.9 31.5 %all_to_all.25.in_ref = bf16[32,2,768]{2,1,0:T(2,128)(2,1)S(1)} all-to-all(bf16[32,2,768]{2,1,0:T(2,128)(2,1)} %get-tuple-element.19), channel_id=1, replica_groups=mesh['ep_hi'=4,'ep_lo'=4,'core'=2,'tp'=16] {'ep_hi','ep_lo','core'}, dimensions={0} | all-to-all | bytes 196608 | tf_op jit(solution)/shard_map/all_to_all | solution.py:444
  34.4 1.9 %shard_map.206 = (bf16[16,320,128]{2,1,0:T(8,128)(2,1)S(1)}, bf16[64,128]{1,0:T(8,128)(2,1)S(1)}) custom-call(bf16[32,2,768]{2,1,0:T(2,128)(2,1)S(1)} %all_to_all.25.in_ref), custom_call_target="tpu_custom_call" | custom-call | flops 655360 | bytes 1425408 | tf_op jit(solution)/shard_map/pallas_call | solution.py:76
  36.4 25.1 %all_to_all.26.refs_0_ = bf16[16,320,128]{2,1,0:T(8,128)(2,1)S(1)} all-to-all(bf16[16,320,128]{2,1,0:T(8,128)(2,1)S(1)} %get-tuple-element.21), channel_id=1, replica_groups=mesh['ep_hi'=4,'ep_lo'=4,'core'=2,'tp'=16] {'tp'}, dimensions={0} | all-to-all | bytes 2621440 | tf_op jit(solution)/shard_map/all_to_all | solution.py:444
  61.5 2.5 %shard_map.211 = bf16[16,320,128]{2,1,0:T(8,128)(2,1)} custom-call(bf16[16,320,128]{2,1,0:T(8,128)(2,1)S(1)} %all_to_all.26.refs_0_, bf16[2048,128]{1,0:T(8,128)(2,1)S(1)} %bitcast.18, bf16[2048,128]{1,0:T(8,128)(2,1)S(1)} %bitcast.19, bf16[128,2048]{1,0:T(8,128)(2,1)S(1)} %bitcast.20), custom_call_target="tpu_custom_call" | custom-call | flops 503316480 | bytes 4194304 | tf_op jit(solution)/shard_map/pallas_call | solution.py:76
  64.0 3.7 %all-to-all-start.3 = ((bf16[16,320,128]{2,1,0:T(8,128)(2,1)}), bf16[16,320,128]{2,1,0:T(8,128)(2,1)S(1)}, u32[]{:S(2)}, u32[]{:S(2)}) async-start(bf16[16,320,128]{2,1,0:T(8,128)(2,1)} %shard_map.211), calls=%async_computation.3 | async-start | bytes 2621440 | tf_op jit(solution)/shard_map/all_to_all | solution.py:444
  67.8 4.4 %collective-permute-start = (bf16[24,256]{1,0:T(8,128)(2,1)S(1)}, bf16[24,256]{1,0:T(8,128)(2,1)S(1)}, u32[]{:S(2)}, u32[]{:S(2)}) collective-permute-start(bf16[24,256]{1,0:T(8,128)(2,1)S(1)} %copy-done.19), channel_id=1, source_target_pairs={{0,16},{16,32},{32,48},{48,64},{64,80},{80,96},{96,112},{112,128},... | collective-permute-start | bytes 36872 | tf_op jit(solution)/shard_map/ppermute | solution.py:499
  72.2 0.8 collective-permute-done.refs_2_.prior_ref
  73.1 0.6 copy-done.9
  73.7 3.5 %shard_map.204 = (bf16[256,256]{1,0:T(8,128)(2,1)}, bf16[256,256]{1,0:T(8,128)(2,1)}, f32[256,128]{1,0:T(8,128)}, bf16[272,128]{1,0:T(8,128)(2,1)}) custom-call(bf16[256,256]{1,0:T(8,128)(2,1)} %refs_0_.3, bf16[256,256]{1,0:T(8,128)(2,1)} %refs_1_.1, bf16[24,256]{1,0:T(8,128)(2,1)} %copy-done.9, bf16[4,256]{1,0:T(4,128)(2,1)} %refs_3_.3, ...), custom_call_target="tpu_custom_call" | custom-call | flops 16777216 | bytes 749584 | tf_op jit(solution)/shard_map/pallas_call | solution.py:76
  77.2 2.2 %all-gather = bf16[544,128]{1,0:T(8,128)(2,1)S(1)} all-gather(bf16[272,128]{1,0:T(8,128)(2,1)} %get-tuple-element.16), channel_id=2, replica_groups=mesh['ep_hi'=4,'ep_lo'=4,'core'=2,'tp'=16] {'core'}, dimensions={0}, use_global_device_ids=true | all-gather | bytes 208896 | tf_op jit(solution)/shard_map/all_gather | solution.py:530
  79.4 0.2 shard_map.205
  79.6 14.7 %all-gather.1 = bf16[512,128]{1,0:T(8,128)(2,1)S(1)} all-gather(bf16[128,128]{1,0:T(8,128)(2,1)S(1)} %get-tuple-element.17), channel_id=3, replica_groups=mesh['ep_hi'=4,'ep_lo'=4,'core'=2,'tp'=16] {'ep_hi'}, dimensions={0}, use_global_device_ids=true | all-gather | bytes 163840 | tf_op jit(solution)/shard_map/all_gather | solution.py:533
  94.4 0.2 shard_map.207
  94.6 12.1 %all-gather.2 = bf16[8,144,128]{2,1,0:T(8,128)(2,1)S(1)} all-gather(bf16[2,144,128]{2,1,0:T(8,128)(2,1)S(1)} %shard_map.207), channel_id=4, replica_groups=mesh['ep_hi'=4,'ep_lo'=4,'core'=2,'tp'=16] {'ep_lo'}, dimensions={0}, use_global_device_ids=true | all-gather | bytes 368640 | tf_op jit(solution)/shard_map/all_gather | solution.py:537
  106.9 7.9 %all_gather.27.chips_ref = f32[256,128]{1,0:T(8,128)S(1)} all-gather(f32[128,128]{1,0:T(8,128)S(1)} %shard_map.208), channel_id=1, replica_groups=mesh['ep_hi'=4,'ep_lo'=4,'core'=2,'tp'=16] {'core'}, dimensions={0}, use_global_device_ids=true | all-gather | bytes 196608 | tf_op jit(solution)/shard_map/all_gather | solution.py:539
  114.9 3.1 %shard_map.209 = bf16[16,256,128]{2,1,0:T(8,128)(2,1)} custom-call(bf16[256,256]{1,0:T(8,128)(2,1)S(1)} %copy-done.6, bf16[256,256]{1,0:T(8,128)(2,1)S(1)} %copy-done.7, bf16[256,256]{1,0:T(8,128)(2,1)S(1)} %copy-done.1, bf16[24,256]{1,0:T(8,128)(2,1)S(1)} %copy-done.10, bf16[4,256]{1,0:T(4,128)(2,1)S(1)} %copy-done.15, bf16[256,256]{1,0:T(8,128)(2,1)S(1)} %copy-done.5, ...), custom_call_target="tpu_custom_call" | custom-call | flops 268435456 | bytes 3046432 | tf_op jit(solution)/shard_map/pallas_call | solution.py:76
  118.0 6.5 %all-to-all-start.1 = ((bf16[16,256,128]{2,1,0:T(8,128)(2,1)}), bf16[16,256,128]{2,1,0:T(8,128)(2,1)S(1)}, u32[]{:S(2)}, u32[]{:S(2)}) async-start(bf16[16,256,128]{2,1,0:T(8,128)(2,1)} %shard_map.209), calls=%async_computation.1 | async-start | bytes 2097152 | tf_op jit(solution)/shard_map/all_to_all | solution.py:444
  124.6 0.9 shard_map.212
  125.4 15.4 %all-to-all-done.1.in_ref = bf16[16,256,128]{2,1,0:T(8,128)(2,1)S(1)} async-done(((bf16[16,256,128]{2,1,0:T(8,128)(2,1)}), bf16[16,256,128]{2,1,0:T(8,128)(2,1)S(1)}, u32[]{:S(2)}, u32[]{:S(2)}) %all-to-all-start.1) | async-done | bytes 1048608 | tf_op jit(solution)/shard_map/all_to_all | solution.py:444
  140.9 8.9 %all-to-all-start.4 = ((bf16[32,2,640]{2,1,0:T(2,128)(2,1)}), bf16[32,2,640]{2,1,0:T(2,128)(2,1)S(1)}, u32[]{:S(2)}, u32[]{:S(2)}) async-start(bf16[32,2,640]{2,1,0:T(2,128)(2,1)} %shard_map.212), calls=%async_computation.4 | async-start | bytes 163840 | tf_op jit(solution)/shard_map/all_to_all | solution.py:444
  149.8 0.8 shard_map.210
  150.6 12.9 %all-to-all-done.4.table_ref = bf16[32,2,640]{2,1,0:T(2,128)(2,1)S(1)} async-done(((bf16[32,2,640]{2,1,0:T(2,128)(2,1)}), bf16[32,2,640]{2,1,0:T(2,128)(2,1)S(1)}, u32[]{:S(2)}, u32[]{:S(2)}) %all-to-all-start.4) | async-done | bytes 81952 | tf_op jit(solution)/shard_map/all_to_all | solution.py:444
  163.5 1.5 shard_map.213
  (41 shorter events, 0.3 us)
Async XLA Ops:
  36.3 25.1 %copy-start.2 = (bf16[1,2048,128]{2,1,0:T(8,128)(2,1)S(1)}, bf16[1,2048,128]{2,1,0:T(8,128)(2,1)}, u32[]{:S(2)}) copy-start(bf16[1,2048,128]{2,1,0:T(8,128)(2,1)} %param.37) | copy-start | bytes 1572868
  36.4 25.1 %copy-start.3 = (bf16[1,2048,128]{2,1,0:T(8,128)(2,1)S(1)}, bf16[1,2048,128]{2,1,0:T(8,128)(2,1)}, u32[]{:S(2)}) copy-start(bf16[1,2048,128]{2,1,0:T(8,128)(2,1)} %param.38) | copy-start | bytes 1572868
  36.4 25.1 %copy-start.4 = (bf16[1,128,2048]{2,1,0:T(8,128)(2,1)S(1)}, bf16[1,128,2048]{2,1,0:T(8,128)(2,1)}, u32[]{:S(2)}) copy-start(bf16[1,128,2048]{2,1,0:T(8,128)(2,1)} %param.39) | copy-start | bytes 1572868
  64.0 3.8 %copy-start.19 = (bf16[24,256]{1,0:T(8,128)(2,1)S(1)}, bf16[24,256]{1,0:T(8,128)(2,1)}, u32[]{:S(2)}) copy-start(bf16[24,256]{1,0:T(8,128)(2,1)} %get-tuple-element.12) | copy-start | bytes 36868
  64.0 54.0 %all-to-all-start.3 = ((bf16[16,320,128]{2,1,0:T(8,128)(2,1)}), bf16[16,320,128]{2,1,0:T(8,128)(2,1)S(1)}, u32[]{:S(2)}, u32[]{:S(2)}) async-start(bf16[16,320,128]{2,1,0:T(8,128)(2,1)} %shard_map.211), calls=%async_computation.3 | async-start | bytes 2621440 | tf_op jit(solution)/shard_map/all_to_all | solution.py:444
  67.7 47.1 %copy-start = (bf16[256,2048]{1,0:T(8,128)(2,1)S(1)}, bf16[256,2048]{1,0:T(8,128)(2,1)}, u32[]{:S(2)}) copy-start(bf16[256,2048]{1,0:T(8,128)(2,1)} %weight_ref.1) | copy-start | bytes 3145732
  67.7 47.1 %copy-start.1 = (bf16[256,256]{1,0:T(8,128)(2,1)S(1)}, bf16[256,256]{1,0:T(8,128)(2,1)}, u32[]{:S(2)}) copy-start(bf16[256,256]{1,0:T(8,128)(2,1)} %projection_ref.1) | copy-start | bytes 393220
  67.7 47.0 %copy-start.5 = (bf16[256,256]{1,0:T(8,128)(2,1)S(1)}, bf16[256,256]{1,0:T(8,128)(2,1)}, u32[]{:S(2)}) copy-start(bf16[256,256]{1,0:T(8,128)(2,1)} %gate_ref.1) | copy-start | bytes 393220
  67.8 47.0 %copy-start.11 = (f32[256,4]{0,1:T(4,128)S(1)}, f32[256,4]{0,1:T(4,128)}, u32[]{:S(2)}) copy-start(f32[256,4]{0,1:T(4,128)} %param.24) | copy-start | bytes 12292
  67.8 47.0 %copy-start.12 = (f32[256,4]{0,1:T(4,128)S(1)}, f32[256,4]{0,1:T(4,128)}, u32[]{:S(2)}) copy-start(f32[256,4]{0,1:T(4,128)} %param.25) | copy-start | bytes 12292
  67.8 47.0 %copy-start.13 = (f32[4]{0:T(128)S(1)}, f32[4]{0:T(128)}, u32[]{:S(2)}) copy-start(f32[4]{0:T(128)} %param.29) | copy-start | bytes 52
  67.8 47.0 %copy-start.15 = (bf16[4,256]{1,0:T(4,128)(2,1)S(1)}, bf16[4,256]{1,0:T(4,128)(2,1)}, u32[]{:S(2)}) copy-start(bf16[4,256]{1,0:T(4,128)(2,1)} %taps_ref.1) | copy-start | bytes 6148
  67.8 47.0 %copy-start.16 = (f32[256]{0:T(256)S(1)}, f32[256]{0:T(256)}, u32[]{:S(2)}) copy-start(f32[256]{0:T(256)} %param.31) | copy-start | bytes 3076
  67.8 47.0 %copy-start.18 = (f32[4]{0:T(128)S(1)}, f32[4]{0:T(128)}, u32[]{:S(2)}) copy-start(f32[4]{0:T(128)} %param.30) | copy-start | bytes 52
  67.8 5.2 %collective-permute-start = (bf16[24,256]{1,0:T(8,128)(2,1)S(1)}, bf16[24,256]{1,0:T(8,128)(2,1)S(1)}, u32[]{:S(2)}, u32[]{:S(2)}) collective-permute-start(bf16[24,256]{1,0:T(8,128)(2,1)S(1)} %copy-done.19), channel_id=1, source_target_pairs={{0,16},{16,32},{32,48},{48,64},{64,80},{80,96},{96,112},{112,128},... | collective-permute-start | bytes 36872 | tf_op jit(solution)/shard_map/ppermute | solution.py:499
  73.1 0.6 copy-start.9
  77.1 37.7 %copy-start.6 = (bf16[256,256]{1,0:T(8,128)(2,1)S(1)}, bf16[256,256]{1,0:T(8,128)(2,1)}, u32[]{:S(2)}) copy-start(bf16[256,256]{1,0:T(8,128)(2,1)} %get-tuple-element.13.x_ref) | copy-start | bytes 393220
  77.1 37.7 %copy-start.7 = (bf16[256,256]{1,0:T(8,128)(2,1)S(1)}, bf16[256,256]{1,0:T(8,128)(2,1)}, u32[]{:S(2)}) copy-start(bf16[256,256]{1,0:T(8,128)(2,1)} %get-tuple-element.14.b_ref) | copy-start | bytes 393220
  77.1 37.7 %copy-start.8 = (f32[256,128]{1,0:T(8,128)S(1)}, f32[256,128]{1,0:T(8,128)}, u32[]{:S(2)}) copy-start(f32[256,128]{1,0:T(8,128)} %get-tuple-element.15.first_ref) | copy-start | bytes 393220
  77.2 37.7 %copy-start.10 = (bf16[24,256]{1,0:T(8,128)(2,1)S(1)}, bf16[24,256]{1,0:T(8,128)(2,1)}, u32[]{:S(2)}) copy-start(bf16[24,256]{1,0:T(8,128)(2,1)} %copy-done.9) | copy-start | bytes 36868
  118.0 22.9 %all-to-all-start.1 = ((bf16[16,256,128]{2,1,0:T(8,128)(2,1)}), bf16[16,256,128]{2,1,0:T(8,128)(2,1)S(1)}, u32[]{:S(2)}, u32[]{:S(2)}) async-start(bf16[16,256,128]{2,1,0:T(8,128)(2,1)} %shard_map.209), calls=%async_computation.1 | async-start | bytes 2097152 | tf_op jit(solution)/shard_map/all_to_all | solution.py:444
  124.5 39.0 %copy-start.14 = (s32[128,2]{0,1:T(2,128)S(1)}, s32[128,2]{0,1:T(2,128)}, u32[]{:S(2)}) copy-start(s32[128,2]{0,1:T(2,128)} %param.34) | copy-start | bytes 3076
  124.6 39.0 %copy-start.17 = (f32[128,2]{0,1:T(2,128)S(1)}, f32[128,2]{0,1:T(2,128)}, u32[]{:S(2)}) copy-start(f32[128,2]{0,1:T(2,128)} %param.35) | copy-start | bytes 3076
  140.9 22.6 %all-to-all-start.4 = ((bf16[32,2,640]{2,1,0:T(2,128)(2,1)}), bf16[32,2,640]{2,1,0:T(2,128)(2,1)S(1)}, u32[]{:S(2)}, u32[]{:S(2)}) async-start(bf16[32,2,640]{2,1,0:T(2,128)(2,1)} %shard_map.212), calls=%async_computation.4 | async-start | bytes 163840 | tf_op jit(solution)/shard_map/all_to_all | solution.py:444
